TPU v7x, 32 devices: a whole 2x2x4 slice. The times are simulated.
32 devices in a mesh: rep: 2 (over x), fs: 8 (over z, y), tp: 2 (over core).
Axes of the slice: x: 2, y: 2, z: 4, core: 2. Of those that a mesh axis runs over, the one named last changes fastest.
Arguments:
- gate_late: bfloat16 [6144, 4096], P(('rep', 'fs'), 'tp'), may hold values from -6 to 6
- up_late: bfloat16 [6144, 4096], P(('rep', 'fs'), 'tp'), may hold values from -6 to 6
- gate_early: bfloat16 [6144, 4096], P(('rep', 'fs'), 'tp'), may hold values from -6 to 6
- up_early: bfloat16 [6144, 4096], P(('rep', 'fs'), 'tp'), may hold values from -6 to 6
- cotangent: bfloat16 [6144, 2048], P(('rep', 'fs')), may hold values from -6 to 6
- w_down: bfloat16 [2048, 4096], P('fs', 'tp'), may hold values from -0.09375 to 0.09375
- grad_in: float32 [2048, 4096], P('fs', 'tp'), may hold values from -6 to 6
Outputs:
- late_out: bfloat16 [6144, 2048], P(('rep', 'fs'))
- gate_grad: bfloat16 [6144, 4096], P(('rep', 'fs'), 'tp')
- up_grad: bfloat16 [6144, 4096], P(('rep', 'fs'), 'tp')
- grad_out: float32 [2048, 4096], P('fs', 'tp')
All inputs are finite; a program needn't handle non-finite values.
Results may differ from a plain program's by a relative error of at most 0.014.
Values may be sent and summed in bfloat16 or wider, within the bound.
A program may use at most 64 MiB of HBM per device.

v0:
```python
import functools
import math

import jax
import jax.numpy as jnp
from jax import lax
from jax.experimental import pallas as pl
from jax.experimental.pallas import tpu as pltpu
from jax.sharding import PartitionSpec as P

MESH = pl.DeviceIdType.MESH
F32 = jnp.float32
BF16 = jnp.bfloat16
LINK_ROWS = 16


def ring_place(index, count):
    odd = lax.rem(index, 2)
    half = lax.div(index, 2)
    return (1 - odd) * half + odd * (count - 1 - half)


def ring_index(place, count):
    place = lax.rem(place + 2 * count, count)
    back = lax.div(place, count // 2)
    return (1 - back) * 2 * place + back * (2 * (count - 1 - place) + 1)


def kernel(
    n, n_tp, qa, qr, scale,
    gl, ul, ge, ue, cot, w, gin,
    late, gg, ug, gout,
    wf, lacc, hg, contrib, rs_s, rs_r, xr_s, xr_r, hl, he, part, fin_s, fin_r,
    ag_ss, ag_rs, xf_ss, xf_rs, rs_ss, rs_rs, xr_ss, xr_rs, fin_ss, fin_rs, tp_ss, tp_rs,
):
    tokens, cols = gl.shape
    rows = w.shape[0]
    half = cols // 2
    rep = lax.axis_index("rep")
    me = lax.axis_index("fs")
    tp = lax.axis_index("tp")
    place = ring_place(me, n)
    right = ring_index(place + 1, n)
    left = ring_index(place + n - 1, n)
    other = 1 - rep

    barrier = pltpu.get_barrier_semaphore()
    for target in (right, left):
        pl.semaphore_signal(barrier, inc=1, device_id={"fs": target}, device_id_type=MESH)
    pl.semaphore_signal(barrier, inc=1, device_id={"rep": other}, device_id_type=MESH)
    for k in range(1, n_tp):
        pl.semaphore_signal(
            barrier, inc=1, device_id={"tp": lax.rem(tp + k, n_tp)}, device_id_type=MESH
        )
    pl.semaphore_wait(barrier, 2 + n_tp)

    lanes = (pl.ds(0, half), pl.ds(half, half))
    towards = (right, left)

    def shard_at(way, step):
        return ring_index(place - step if way == 0 else place + step, n)

    def columns(ref, shard):
        if len(ref.shape) == 3:
            return ref[shard]
        return ref[:, pl.ds(pl.multiple_of(shard * rows, rows), rows)]

    def aligned(value):
        return pl.multiple_of(value, LINK_ROWS)

    ag_rows = pl.ds(aligned(rep * qa), rows - qa)
    ag_mine = pl.ds(aligned(rep * (rows - qa)), qa)
    ag_theirs = pl.ds(aligned(other * (rows - qa)), qa)
    rs_rows = pl.ds(aligned(rep * qr), rows - qr)
    rs_theirs = pl.ds(aligned(other * (rows - qr)), qr)
    rs_within = pl.ds(aligned(rep * (rows - 2 * qr)), qr)

    def gather(way, step, first=False):
        shard = shard_at(way, step)
        spot = wf.at[shard, ag_rows, lanes[way]]
        return pltpu.make_async_remote_copy(
            src_ref=w.at[ag_rows, lanes[way]] if first else spot,
            dst_ref=spot,
            send_sem=ag_ss.at[way, step],
            recv_sem=ag_rs.at[way, step],
            device_id={"fs": towards[way]},
            device_id_type=MESH,
        )

    def gather_wait(way, step):
        spot = wf.at[shard_at(way, step + 1), ag_rows, lanes[way]]
        pltpu.make_async_remote_copy(
            src_ref=spot, dst_ref=spot, send_sem=ag_ss.at[way, step],
            recv_sem=ag_rs.at[way, step], device_id={"fs": towards[way]}, device_id_type=MESH,
        ).wait_recv()

    def cross(way, step, span):
        spot = wf.at[shard_at(way, step + 1), span, lanes[way]]
        return pltpu.make_async_remote_copy(
            src_ref=spot, dst_ref=spot, send_sem=xf_ss.at[way, step],
            recv_sem=xf_rs.at[way, step], device_id={"rep": other}, device_id_type=MESH,
        )

    def reduce_copy(way, step):
        return pltpu.make_async_remote_copy(
            src_ref=rs_s.at[way, step], dst_ref=rs_r.at[way, step],
            send_sem=rs_ss.at[way, step], recv_sem=rs_rs.at[way, step],
            device_id={"fs": towards[way]}, device_id_type=MESH,
        )

    def pair_copy(way, step):
        return pltpu.make_async_remote_copy(
            src_ref=xr_s.at[way, step], dst_ref=xr_r.at[way, step],
            send_sem=xr_ss.at[way, step], recv_sem=xr_rs.at[way, step],
            device_id={"rep": other}, device_id_type=MESH,
        )

    for way in range(2):
        gather(way, 0, first=True).start()

    tile = 16

    @pl.loop(0, tokens // tile)
    def _(i):
        span = pl.ds(pl.multiple_of(i * tile, tile), tile)
        gate = ge[span, :].astype(F32)
        he[span, :] = (gate * (1.0 / (1.0 + jnp.exp(-gate))) * ue[span, :].astype(F32)).astype(BF16)

    def own_share(way, step):
        shard = shard_at(way, step + 1)
        contrib[way] = lax.dot_general(
            columns(cot, shard), he[:, lanes[way]], (((0,), (0,)), ((), ())),
            preferred_element_type=F32,
        )
        xr_s[way, step] = contrib[way, rs_theirs, :].astype(BF16)
        pair_copy(way, step).start()

    def running(way, step):
        pair_copy(way, step).wait_recv()
        contrib[way, pl.ds(aligned(rep * (rows - qr)), qr), :] += xr_r[way, step].astype(F32)

    for way in range(2):
        own_share(way, 0)

    @pl.loop(0, tokens // tile)
    def _(i):
        span = pl.ds(pl.multiple_of(i * tile, tile), tile)
        gate = gl[span, :].astype(F32)
        hl[span, :] = (gate * (1.0 / (1.0 + jnp.exp(-gate))) * ul[span, :].astype(F32)).astype(BF16)
        hg[span, :] = jnp.zeros((tile, cols), F32)

    wf[me] = w[...]

    @pl.loop(0, n)
    def _(k):
        lacc[k] = jnp.zeros((tokens, rows), F32)

    for way in range(2):
        running(way, 0)
        rs_s[way, 0] = contrib[way, rs_rows, :].astype(BF16)
        reduce_copy(way, 0).start()

    def use(way, step):
        shard = shard_at(way, step)
        block = wf[shard, :, lanes[way]]
        lacc[shard] += lax.dot_general(
            hl[:, lanes[way]], block, (((1,), (1,)), ((), ())), preferred_element_type=F32
        )
        hg[:, lanes[way]] += jnp.dot(columns(cot, shard), block, preferred_element_type=F32)

    final = pltpu.make_async_remote_copy(
        src_ref=fin_s, dst_ref=fin_r, send_sem=fin_ss, recv_sem=fin_rs,
        device_id={"rep": other}, device_id_type=MESH,
    )

    def advance(step, last):
        for way in range(2):
            own_share(way, step + 1)
        for way in range(2):
            running(way, step + 1)
            reduce_copy(way, step).wait_recv()
            total = contrib[way, rs_rows, :] + rs_r[way, step].astype(F32)
            if last:
                fin_s[:, lanes[way]] = total.astype(BF16)
            else:
                rs_s[way, step + 1] = total.astype(BF16)
                reduce_copy(way, step + 1).start()
        if last:
            final.start()
        for way in range(2):

            @pl.when(step >= 1)
            def _():
                cross(way, step - 1, ag_theirs).wait_recv()

            use(way, step)
        for way in range(2):
            gather_wait(way, step)
            if not last:
                gather(way, step + 1).start()
            cross(way, step, ag_mine).start()

    def body(step, carry):
        advance(step, False)
        return carry

    lax.fori_loop(0, n - 2, body, 0)
    advance(jnp.int32(n - 2), True)

    for way in range(2):
        cross(way, n - 2, ag_theirs).wait_recv()
        use(way, n - 1)

    @pl.loop(0, n)
    def _(k):
        part[tp, k] = lacc[k].astype(BF16)

    def share(k):
        return pltpu.make_async_remote_copy(
            src_ref=part.at[tp], dst_ref=part.at[tp], send_sem=tp_ss.at[k], recv_sem=tp_rs.at[k],
            device_id={"tp": lax.rem(tp + k, n_tp)}, device_id_type=MESH,
        )

    def share_wait(k):
        spot = part.at[lax.rem(tp + n_tp - k, n_tp)]
        pltpu.make_async_remote_copy(
            src_ref=spot, dst_ref=spot, send_sem=tp_ss.at[k], recv_sem=tp_rs.at[k],
            device_id={"tp": lax.rem(tp + k, n_tp)}, device_id_type=MESH,
        ).wait_recv()

    for k in range(1, n_tp):
        share(k).start()

    @pl.loop(0, tokens // tile)
    def _(i):
        span = pl.ds(pl.multiple_of(i * tile, tile), tile)
        gate = ge[span, :].astype(F32)
        sig = 1.0 / (1.0 + jnp.exp(-gate))
        grad = hg[span, :]
        ug[span, :] = (grad * (gate * sig)).astype(BF16)
        gg[span, :] = (
            grad * ue[span, :].astype(F32) * sig * (1.0 + gate * (1.0 - sig))
        ).astype(BF16)

    for k in range(1, n_tp):
        share_wait(k)

    @pl.loop(0, n)
    def _(k):
        total = part[0, k].astype(F32)
        for j in range(1, n_tp):
            total = total + part[j, k].astype(F32)
        if len(late.shape) == 3:
            late[k] = total.astype(BF16)
        else:
            late[:, pl.ds(pl.multiple_of(k * rows, rows), rows)] = total.astype(BF16)

    final.wait_recv()
    shared = rows - 2 * qr
    mine_only = pl.ds(aligned(rep * (rows - qr)), qr)
    theirs_only = pl.ds(aligned(other * (rows - qr)), qr)
    gout[mine_only, :] = gin[mine_only, :] + fin_s[rs_within, :].astype(F32) * scale
    gout[theirs_only, :] = (
        gin[theirs_only, :] + fin_r[pl.ds(aligned(other * shared), qr), :].astype(F32) * scale
    )
    if shared:
        both = pl.ds(qr, shared)
        gout[both, :] = gin[both, :] + scale * (
            fin_s[pl.ds(aligned(other * qr), shared), :].astype(F32)
            + fin_r[pl.ds(aligned(rep * qr), shared), :].astype(F32)
        )

    final.wait_send()
    for k in range(1, n_tp):
        share(k).wait_send()
    for way in range(2):
        gather(way, 0, first=True).wait_send()
        pair_copy(way, n - 1).wait_send()

    @pl.loop(0, n - 1)
    def _(step):
        for way in range(2):
            cross(way, step, ag_mine).wait_send()
            reduce_copy(way, step).wait_send()
            pair_copy(way, step).wait_send()

    @pl.loop(1, n - 1)
    def _(step):
        for way in range(2):
            gather(way, step).wait_send()


def solution(mesh):
    n, n_tp, n_rep = mesh.shape["fs"], mesh.shape["tp"], mesh.shape["rep"]
    assert n_rep == 2 and n % 2 == 0 and n > 2

    def per_device(gl, ul, ge, ue, cotangent, w, gin):
        tokens, cols = gl.shape
        rows, width = w.shape[0], cotangent.shape[1]
        half = cols // 2
        qa = (rows * 3 // 16) // LINK_ROWS * LINK_ROWS
        qr = (rows * 6 // 16) // LINK_ROWS * LINK_ROWS
        scale = 1.0 / math.sqrt(tokens * n_rep * n)
        whole_lanes = rows % 128 == 0
        cot = cotangent
        if not whole_lanes:
            cot = cotangent.reshape(tokens, n, rows).transpose(1, 0, 2)
        vmem = pl.BlockSpec(memory_space=pltpu.VMEM)
        dma = pltpu.SemaphoreType.DMA
        late, gg, ug, gout = pl.pallas_call(
            functools.partial(kernel, n, n_tp, qa, qr, scale),
            out_shape=(
                jax.ShapeDtypeStruct(cot.shape, BF16),
                jax.ShapeDtypeStruct((tokens, cols), BF16),
                jax.ShapeDtypeStruct((tokens, cols), BF16),
                jax.ShapeDtypeStruct((rows, cols), F32),
            ),
            in_specs=[vmem] * 7,
            out_specs=(vmem,) * 4,
            scratch_shapes=[
                pltpu.VMEM((n, rows, cols), BF16),
                pltpu.VMEM((n, tokens, rows), F32),
                pltpu.VMEM((tokens, cols), F32),
                pltpu.VMEM((2, rows, half), F32),
                pltpu.VMEM((2, n - 1, rows - qr, half), BF16),
                pltpu.VMEM((2, n - 1, rows - qr, half), BF16),
                pltpu.VMEM((2, n, qr, half), BF16),
                pltpu.VMEM((2, n, qr, half), BF16),
                pltpu.VMEM((tokens, cols), BF16),
                pltpu.VMEM((tokens, cols), BF16),
                pltpu.VMEM((n_tp, n, tokens, rows), BF16),
                pltpu.VMEM((rows - qr, cols), BF16),
                pltpu.VMEM((rows - qr, cols), BF16),
            ]
            + [dma((2, n))] * 8
            + [dma, dma, dma((n_tp,)), dma((n_tp,))],
            compiler_params=pltpu.CompilerParams(
                collective_id=0, has_side_effects=True, vmem_limit_bytes=67043328
            ),
        )(gl, ul, ge, ue, cot, w, gin)
        if not whole_lanes:
            late = late.transpose(1, 0, 2).reshape(tokens, width)
        return late, gg, ug, gout

    placed = (
        P(("rep", "fs"), "tp"),
        P(("rep", "fs"), "tp"),
        P(("rep", "fs"), "tp"),
        P(("rep", "fs"), "tp"),
        P(("rep", "fs"), None),
        P("fs", "tp"),
        P("fs", "tp"),
    )
    return jax.shard_map(
        per_device,
        mesh=mesh,
        in_specs=placed,
        out_specs=(
            P(("rep", "fs"), None),
            P(("rep", "fs"), "tp"),
            P(("rep", "fs"), "tp"),
            P("fs", "tp"),
        ),
        check_vma=False,
    )
```

profile of v0, /device:TPU:0, one launch (start us, length us, event | category | flops | bytes accessed | tf_op | source)
XLA Modules:
  0.0 157.3 jit_solution(12043335552047940736)
XLA Ops:
  0.6 148.4 %shard_map.102 = (bf16[384,2048]{1,0:T(8,128)(2,1)}, bf16[384,2048]{1,0:T(8,128)(2,1)}, bf16[384,2048]{1,0:T(8,128)(2,1)}, f32[256,2048]{1,0:T(8,128)}) custom-call(bf16[384,2048]{1,0:T(8,128)(2,1)} %gl.1, bf16[384,2048]{1,0:T(8,128)(2,1)} %ul.1, bf16[384,2048]{1,0:T(8,128)(2,1)} %ge.1, bf16[384,2048]{1,0:T(8,128)(2,1)} %ue.1, bf16[384,2048]{1,0:T(8,128)(2,1)} %cot.1, ...), custom_call_target="tpu_custom_call" | custom-call | tf_op jit(solution)/shard_map/pallas_call | solution.py:310
  149.0 0.0 copy-start.2
  149.0 2.8 %copy.15 = bf16[384,2048]{1,0:T(8,128)(2,1)} copy(bf16[384,2048]{1,0:T(8,128)(2,1)} %get-tuple-element.8) | data formatting | bytes 3145728
  151.9 0.0 copy-done.2
  151.9 0.0 copy-start.1
  151.9 1.1 copy.16
  153.0 0.8 copy-done.1
  153.9 0.0 copy-start
  153.9 1.1 copy.17
  155.0 1.0 copy-done
  156.0 1.3 copy.18
Async XLA Ops:
  149.0 2.9 %copy-start.2 = (bf16[384,2048]{1,0:T(8,128)(2,1)S(1)}, bf16[384,2048]{1,0:T(8,128)(2,1)}, u32[]{:S(2)}) copy-start(bf16[384,2048]{1,0:T(8,128)(2,1)} %get-tuple-element.9) | copy-start | bytes 4718596
  151.9 2.0 %copy-start.1 = (bf16[384,2048]{1,0:T(8,128)(2,1)S(1)}, bf16[384,2048]{1,0:T(8,128)(2,1)}, u32[]{:S(2)}) copy-start(bf16[384,2048]{1,0:T(8,128)(2,1)} %get-tuple-element.10) | copy-start | bytes 4718596
  153.9 2.2 %copy-start = (f32[256,2048]{1,0:T(8,128)S(1)}, f32[256,2048]{1,0:T(8,128)}, u32[]{:S(2)}) copy-start(f32[256,2048]{1,0:T(8,128)} %get-tuple-element.11) | copy-start | bytes 6291460
where the time goes:
time: 158 us; the launch traced here: 157 us
  Pallas kernels  148 us (94%)
  local copies, waits for them, and re-layouts  8.3 us (5%)
    pallas_call x1, Pallas kernels, per_device(): pl.pallas_call(functools.partial(kernel, n, n_tp, qa, qr, scale), out_sha...  148 us
    unnamed x10, local copies, waits for them, and re-layouts  8.3 us

commit v1 on v0

v1 whole, which is shorter than its diff:
```python
import functools
import math

import jax
import jax.numpy as jnp
from jax import lax
from jax.experimental import pallas as pl
from jax.experimental.pallas import tpu as pltpu
from jax.sharding import PartitionSpec as P

MESH = pl.DeviceIdType.MESH
F32 = jnp.float32
BF16 = jnp.bfloat16
RIGHT, LEFT, ACROSS, OTHER = 0, 1, 2, 3
LAG = 3
USE_LAG = 6
SUM_LAG = 6
TILE = 16


def kernel(
    n, n_tp, chunks, scale,
    gl_h, ul_h, ge_h, ue_h, cot_h, w_h, gin_h,
    late, gg, ug, gout,
    gl, ul, ge, ue, cot, gin, wf, hl, he, he_out, hg, part, own, opp, ys, yr, zs, zr, yfs, yfr, xs, xr,
    ld, ag_s, ag_r, cx_s, cx_r, ct_s, ct_r, he_s, he_r, y_s, y_r, z_s, z_r, yf_s, yf_r, x_s, x_r, tp_s, tp_r,
):
    tokens, cols = gl.shape
    rows = wf.shape[1]
    quarter = rows // 4
    half = rows // 2
    nz = n // 2
    hq = cols // 2
    width = hq // chunks
    rep = lax.axis_index("rep")
    me = lax.axis_index("fs")
    tp = lax.axis_index("tp")
    z = lax.div(me, 2)
    y = lax.rem(me, 2)
    other = 1 - rep
    flat = len(cot.shape) == 2

    def cot_tokens(ref, start, size):
        return ref.at[pl.ds(start, size), :] if flat else ref.at[:, pl.ds(start, size), :]

    def loads(i):
        pairs = (
            (w_h, wf.at[me]), (cot_h, cot_tokens(cot, 0, tokens)), (ge_h, ge), (ue_h, ue),
            (gl_h, gl), (ul_h, ul), (gin_h, gin),
        )
        return pltpu.make_async_copy(pairs[i][0], pairs[i][1], ld.at[i])

    for i in range(7):
        loads(i).start()

    barrier = pltpu.get_barrier_semaphore()

    @pl.when(z < nz - 1)
    def _():
        pl.semaphore_signal(barrier, inc=1, device_id={"fs": me + 2}, device_id_type=MESH)

    @pl.when(z > 0)
    def _():
        pl.semaphore_signal(barrier, inc=1, device_id={"fs": me - 2}, device_id_type=MESH)

    pl.semaphore_signal(barrier, inc=1, device_id={"fs": 2 * z + 1 - y}, device_id_type=MESH)
    pl.semaphore_signal(barrier, inc=1, device_id={"rep": other}, device_id_type=MESH)
    for k in range(1, n_tp):
        pl.semaphore_signal(barrier, inc=1, device_id={"tp": lax.rem(tp + k, n_tp)}, device_id_type=MESH)
    inner = jnp.where((z > 0) & (z < nz - 1), 1, 0)
    pl.semaphore_wait(barrier, 2 + n_tp + inner)

    def target(way):
        if way == RIGHT:
            return {"fs": me + 2}
        if way == LEFT:
            return {"fs": me - 2}
        if way == ACROSS:
            return {"fs": 2 * z + 1 - y}
        return {"rep": other}

    def piece_rows(p):
        return pl.ds(pl.multiple_of((p + rep * (3 - 2 * p)) * quarter, 16), quarter)

    def piece(way, shard, p):
        spot = wf.at[shard, piece_rows(p), :]
        return pltpu.make_async_remote_copy(
            src_ref=spot, dst_ref=spot, send_sem=ag_s.at[way, shard, p],
            recv_sem=ag_r.at[shard, 3 if way == OTHER else p],
            device_id=target(way), device_id_type=MESH,
        )

    def piece_arrived(shard, p):
        spot = wf.at[shard, piece_rows(p), :]
        pltpu.make_async_remote_copy(
            src_ref=spot, dst_ref=spot, send_sem=ag_s.at[0, shard, 0], recv_sem=ag_r.at[shard, p],
            device_id=target(OTHER), device_id_type=MESH,
        ).wait_recv()

    loads(0).wait()
    for p in range(3):
        piece(ACROSS, me, (2, 0, 1)[p]).start()

        @pl.when(z < nz - 1)
        def _():
            piece(RIGHT, me, p).start()

        @pl.when(z > 0)
        def _():
            piece(LEFT, me, p).start()

    lot = tokens // n_tp

    def cot_cross():
        return pltpu.make_async_remote_copy(
            src_ref=cot_tokens(cot, pl.multiple_of(tp * lot, 16), lot),
            dst_ref=cot_tokens(cot, pl.multiple_of(tokens + tp * lot, 16), lot),
            send_sem=cx_s, recv_sem=cx_r, device_id={"rep": other}, device_id_type=MESH,
        )

    def cot_share(k, sender):
        spot = cot_tokens(cot, pl.multiple_of(tokens + sender * lot, 16), lot)
        return pltpu.make_async_remote_copy(
            src_ref=spot, dst_ref=spot, send_sem=ct_s.at[k], recv_sem=ct_r.at[k],
            device_id={"tp": lax.rem(tp + k, n_tp)}, device_id_type=MESH,
        )

    loads(1).wait()
    cot_cross().start()

    def columns(c):
        return pl.ds(pl.multiple_of(c * width, 128), width)

    def he_cross(c):
        return pltpu.make_async_remote_copy(
            src_ref=he_out.at[:, columns(c)], dst_ref=he.at[pl.ds(tokens, tokens), columns(c)],
            send_sem=he_s.at[c], recv_sem=he_r.at[c], device_id={"rep": other}, device_id_type=MESH,
        )

    def tile_at(i):
        return pl.ds(pl.multiple_of(i * TILE, TILE), TILE)

    def gated(gate_ref, up_ref, span, lanes):
        gate = gate_ref[span, lanes].astype(F32)
        return (gate * (1.0 / (1.0 + jnp.exp(-gate))) * up_ref[span, lanes].astype(F32)).astype(BF16)

    mine_lanes = pl.ds(pl.multiple_of(rep * hq, 128), hq)
    theirs_lanes = pl.ds(pl.multiple_of(other * hq, 128), hq)
    loads(2).wait()
    loads(3).wait()

    @pl.loop(0, tokens // TILE)
    def _(i):
        he_out[tile_at(i), :] = gated(ge, ue, tile_at(i), theirs_lanes)

    for c in range(chunks):
        he_cross(c).start()

    @pl.loop(0, tokens // TILE)
    def _(i):
        he[tile_at(i), :] = gated(ge, ue, tile_at(i), mine_lanes)

    beyond = 2 * z + 1 - y
    piece_arrived(beyond, 2)

    @pl.when(z < nz - 1)
    def _():
        piece(RIGHT, beyond, 2).start()

    @pl.when(z > 0)
    def _():
        piece(LEFT, beyond, 2).start()

    loads(4).wait()
    loads(5).wait()

    @pl.loop(0, tokens // TILE)
    def _(i):
        hl[tile_at(i), :] = gated(gl, ul, tile_at(i), slice(None))
        hg[tile_at(i), :] = jnp.zeros((TILE, cols), F32)

    def nearest(m):
        low = jnp.minimum(z, nz - 1 - z)
        paired = m <= 2 * low
        step = jnp.where(paired, lax.div(m + 1, 2), m - low)
        down = jnp.where(paired, lax.rem(m, 2) == 1, 2 * z > nz - 1)
        return jnp.where(down, z - step, z + step)

    def gather(k):
        hop = lax.div(k, 4) + 1
        p = lax.rem(k, 4)
        line = jnp.where(p == 3, 1 - y, y)
        q = jnp.where(p == 3, 2, p)
        for source, onward, way in ((z - hop, z + 1, RIGHT), (z + hop, z - 1, LEFT)):

            @pl.when((source >= 0) & (source < nz))
            def _():
                shard = 2 * source + line
                piece_arrived(shard, q)

                @pl.when((onward >= 0) & (onward < nz))
                def _():
                    piece(way, shard, q).start()

                @pl.when(p < 2)
                def _():
                    piece(ACROSS, shard, q).start()

                @pl.when(p == 0)
                def _():
                    piece(OTHER, shard, q).start()

    def gather_across(k):
        hop = lax.div(k, 4) + 1
        for source in (z - hop, z + hop):

            @pl.when((source >= 0) & (source < nz))
            def _():
                shard = 2 * source + 1 - y
                piece_arrived(shard, 0)
                piece(OTHER, shard, 0).start()

    def cot_block(first, size, shard):
        if flat:
            return cot[pl.ds(first, size), pl.ds(pl.multiple_of(shard * rows, rows), rows)]
        return cot[shard, pl.ds(first, size), :]

    def share(k, shard):
        return pltpu.make_async_remote_copy(
            src_ref=part.at[tp, shard], dst_ref=part.at[tp, shard],
            send_sem=tp_s.at[k, shard], recv_sem=tp_r.at[k, shard],
            device_id={"tp": lax.rem(tp + k, n_tp)}, device_id_type=MESH,
        )

    def share_arrived(k, shard):
        spot = part.at[lax.rem(tp + n_tp - k, n_tp), shard]
        pltpu.make_async_remote_copy(
            src_ref=spot, dst_ref=spot, send_sem=tp_s.at[k, shard], recv_sem=tp_r.at[k, shard],
            device_id={"tp": lax.rem(tp + k, n_tp)}, device_id_type=MESH,
        ).wait_recv()

    def use(i, carry):
        crossed = lax.rem(i, 2)
        line = jnp.where(crossed == 1, 1 - y, y)
        shard = 2 * nearest(lax.div(i, 2)) + line

        @pl.when(crossed == 1)
        def _():
            piece_arrived(shard, 1)

        @pl.when(i > 0)
        def _():
            piece_arrived(shard, 3)

        block = wf[shard]
        part[tp, shard] = lax.dot_general(
            hl[...], block, (((1,), (1,)), ((), ())), preferred_element_type=F32
        ).astype(BF16)
        for k in range(1, n_tp):
            share(k, shard).start()
        hg[...] += jnp.dot(cot_block(0, tokens, shard), block, preferred_element_type=F32)
        return carry

    def y_copy(c, to):
        return pltpu.make_async_remote_copy(
            src_ref=ys.at[c, to], dst_ref=yr.at[c, to], send_sem=y_s.at[c, to], recv_sem=y_r.at[c, to],
            device_id=target(ACROSS), device_id_type=MESH,
        )

    def z_copy(way, c, to):
        return pltpu.make_async_remote_copy(
            src_ref=zs.at[c, to], dst_ref=zr.at[way, c, to],
            send_sem=z_s.at[c, to], recv_sem=z_r.at[way, c, to],
            device_id=target(way), device_id_type=MESH,
        )

    def z_arrived(way, c, to):
        pltpu.make_async_remote_copy(
            src_ref=zs.at[c, to], dst_ref=zr.at[way, c, to],
            send_sem=z_s.at[c, to], recv_sem=z_r.at[way, c, to],
            device_id=target(OTHER), device_id_type=MESH,
        ).wait_recv()

    def yf_copy(c):
        return pltpu.make_async_remote_copy(
            src_ref=yfs.at[c], dst_ref=yfr.at[c], send_sem=yf_s.at[c], recv_sem=yf_r.at[c],
            device_id=target(ACROSS), device_id_type=MESH,
        )

    def x_copy(c):
        return pltpu.make_async_remote_copy(
            src_ref=xs.at[c], dst_ref=xr.at[c], send_sem=x_s.at[c], recv_sem=x_r.at[c],
            device_id={"rep": other}, device_id_type=MESH,
        )

    def contribute(c):
        he_cross(c).wait_recv()

        @pl.loop(0, nz)
        def _(m):
            to = nearest(nz - 1 - m)

            def term(line):
                return lax.dot_general(
                    cot_block(0, 2 * tokens, 2 * to + line), he[:, columns(c)],
                    (((0,), (0,)), ((), ())), preferred_element_type=F32,
                )

            value = term(1 - y)
            ys[c, to] = value[:half].astype(BF16)
            y_copy(c, to).start()
            opp[c, to] = value[half:]
            own[c, to] = term(y)

    top = pl.ds(0, half)
    mid = pl.ds(half, half)
    low = pl.ds(rows, half)

    def forward(s):
        for way, place in ((RIGHT, z), (LEFT, nz - 1 - z)):
            at = s + jnp.where(place == 0, 1, 0)
            safe = jnp.maximum(at, 0)
            c = lax.div(safe, nz - 1)
            j = lax.rem(safe, nz - 1) - place

            @pl.when((at >= 0) & (at < chunks * (nz - 1)) & (j >= 0))
            def _():
                to = nz - 1 - j if way == RIGHT else j
                y_copy(c, to).wait_recv()

                @pl.when(place == 0)
                def _():
                    zs[c, to, top, :] = (own[c, to, top, :] + yr[c, to].astype(F32)).astype(BF16)
                    zs[c, to, mid, :] = own[c, to, mid, :].astype(BF16)
                    zs[c, to, low, :] = opp[c, to].astype(BF16)

                @pl.when(place > 0)
                def _():
                    z_arrived(way, c, to)
                    before = zr.at[way, c, to]
                    zs[c, to, top, :] = (
                        own[c, to, top, :] + yr[c, to].astype(F32) + before[top, :].astype(F32)
                    ).astype(BF16)
                    zs[c, to, mid, :] = (own[c, to, mid, :] + before[mid, :].astype(F32)).astype(BF16)
                    zs[c, to, low, :] = (opp[c, to] + before[low, :].astype(F32)).astype(BF16)

                z_copy(way, c, to).start()

    def finish_line(c):
        y_copy(c, z).wait_recv()
        own[c, z, top, :] += yr[c, z].astype(F32)
        for way, there in ((RIGHT, z > 0), (LEFT, z < nz - 1)):

            @pl.when(there)
            def _():
                z_arrived(way, c, z)
                before = zr.at[way, c, z]
                opp[c, z] += before[low, :].astype(F32)
                own[c, z] += before[pl.ds(0, rows), :].astype(F32)

        yfs[c] = opp[c, z].astype(BF16)
        yf_copy(c).start()

    def finish_pair(c):
        yf_copy(c).wait_recv()
        own[c, z, mid, :] += yfr[c].astype(F32)
        xs[c] = own[c, z].astype(BF16)
        x_copy(c).start()
        lanes = pl.ds(pl.multiple_of(rep * hq + c * width, 128), width)
        gout[:, lanes] = gin[:, lanes] + own[c, z] * scale

    def finish_cross(c):
        x_copy(c).wait_recv()
        lanes = pl.ds(pl.multiple_of(other * hq + c * width, 128), width)
        gout[:, lanes] = gin[:, lanes] + xr[c].astype(F32) * scale

    def reduce_step(s):
        safe = jnp.maximum(s, 0)
        c = lax.div(safe, nz - 1)
        t = lax.rem(safe, nz - 1)
        ahead = jnp.where(s == -2, 0, c + 1)

        @pl.when(((s == -2) | ((s >= 0) & (t == 0))) & (ahead < chunks))
        def _():
            contribute(ahead)

        forward(s)
        done = c - 1

        @pl.when((t == 0) & (done >= 0) & (done < chunks))
        def _():
            finish_line(done)

        @pl.when((t == 1) & (done >= 0) & (done < chunks))
        def _():
            finish_pair(done)

        @pl.when((t == 2) & (done >= 0) & (done < chunks))
        def _():
            finish_cross(done)

    gather_ticks = 4 * (nz - 1)
    use_ticks = max(2 * n - 3, n + USE_LAG)
    sum_ticks = SUM_LAG + chunks * (nz - 1) + 2

    def used(k):
        return jnp.clip(jnp.minimum(lax.div(k + 2, 2), k - USE_LAG) + 1, 1, n)

    def tick(k, carry):
        @pl.when(k < gather_ticks)
        def _():
            gather(k)

        late_k = k - LAG

        @pl.when((late_k >= 0) & (late_k < gather_ticks) & (lax.rem(jnp.maximum(late_k, 0), 4) == 0))
        def _():
            gather_across(late_k)

        @pl.when(k == 1)
        def _():
            piece_arrived(beyond, 0)
            piece(OTHER, beyond, 0).start()

        @pl.when(k == SUM_LAG - 3)
        def _():
            cot_cross().wait_recv()
            for j in range(1, n_tp):
                cot_share(j, tp).start()

        @pl.when(k == SUM_LAG - 2)
        def _():
            for j in range(1, n_tp):
                cot_share(j, lax.rem(tp + n_tp - j, n_tp)).wait_recv()
            loads(6).wait()

        @pl.when((k >= SUM_LAG - 2) & (k < sum_ticks))
        def _():
            reduce_step(k - SUM_LAG)

        lax.fori_loop(jnp.where(k == 0, 0, used(k - 1)), used(k), use, 0)
        return carry

    lax.fori_loop(0, max(use_ticks, gather_ticks, sum_ticks), tick, 0)

    @pl.loop(0, tokens // TILE)
    def _(i):
        span = tile_at(i)
        gate = ge[span, :].astype(F32)
        sig = 1.0 / (1.0 + jnp.exp(-gate))
        grad = hg[span, :]
        ug[span, :] = (grad * (gate * sig)).astype(BF16)
        gg[span, :] = (
            grad * ue[span, :].astype(F32) * sig * (1.0 + gate * (1.0 - sig))
        ).astype(BF16)

    @pl.loop(0, n)
    def _(shard):
        for k in range(1, n_tp):
            share_arrived(k, shard)
        total = part[0, shard].astype(F32)
        for j in range(1, n_tp):
            total = total + part[j, shard].astype(F32)
        if flat:
            late[:, pl.ds(pl.multiple_of(shard * rows, rows), rows)] = total.astype(BF16)
        else:
            late[shard] = total.astype(BF16)

    reduce_step(jnp.int32(chunks * (nz - 1) + 2))

    cot_cross().wait_send()
    for k in range(1, n_tp):
        cot_share(k, tp).wait_send()
    for p in range(3):
        piece(ACROSS, me, p).wait_send()

    @pl.loop(0, nz)
    def _(at):
        same = 2 * at + y
        crossed = 2 * at + 1 - y

        @pl.when((at <= z) & (z < nz - 1))
        def _():
            for p in range(3):
                piece(RIGHT, same, p).wait_send()
            piece(RIGHT, crossed, 2).wait_send()

        @pl.when((at >= z) & (z > 0))
        def _():
            for p in range(3):
                piece(LEFT, same, p).wait_send()
            piece(LEFT, crossed, 2).wait_send()

        piece(OTHER, crossed, 0).wait_send()

        @pl.when(at != z)
        def _():
            piece(OTHER, same, 0).wait_send()
            for p in range(2):
                piece(ACROSS, same, p).wait_send()

        for k in range(1, n_tp):
            share(k, same).wait_send()
            share(k, crossed).wait_send()

        @pl.loop(0, chunks)
        def _(c):
            y_copy(c, at).wait_send()

            @pl.when(at > z)
            def _():
                z_copy(RIGHT, c, at).wait_send()

            @pl.when(at < z)
            def _():
                z_copy(LEFT, c, at).wait_send()

    @pl.loop(0, chunks)
    def _(c):
        he_cross(c).wait_send()
        yf_copy(c).wait_send()
        x_copy(c).wait_send()


def solution(mesh):
    n, n_tp, n_rep = mesh.shape["fs"], mesh.shape["tp"], mesh.shape["rep"]
    assert n_rep == 2 and n % 2 == 0 and n >= 8

    def per_device(gl, ul, ge, ue, cotangent, w, gin):
        tokens, cols = gl.shape
        rows, width = w.shape[0], cotangent.shape[1]
        assert rows % 64 == 0 and cols % 256 == 0
        nz, hq, half = n // 2, cols // 2, rows // 2
        chunks = 2
        scale = 1.0 / math.sqrt(tokens * n_rep * n)
        whole_lanes = rows % 128 == 0
        cot = cotangent
        if not whole_lanes:
            cot = cotangent.reshape(tokens, n, rows).transpose(1, 0, 2)
        cot_both = (2 * tokens, width) if whole_lanes else (n, 2 * tokens, rows)
        vmem = pl.BlockSpec(memory_space=pltpu.VMEM)
        dma = pltpu.SemaphoreType.DMA
        part = hq // chunks
        late, gg, ug, gout = pl.pallas_call(
            functools.partial(kernel, n, n_tp, chunks, scale),
            out_shape=(
                jax.ShapeDtypeStruct(cot.shape, BF16),
                jax.ShapeDtypeStruct((tokens, cols), BF16),
                jax.ShapeDtypeStruct((tokens, cols), BF16),
                jax.ShapeDtypeStruct((rows, cols), F32),
            ),
            in_specs=[pl.BlockSpec(memory_space=pl.ANY)] * 7,
            out_specs=(vmem,) * 4,
            scratch_shapes=[
                pltpu.VMEM((tokens, cols), BF16),
                pltpu.VMEM((tokens, cols), BF16),
                pltpu.VMEM((tokens, cols), BF16),
                pltpu.VMEM((tokens, cols), BF16),
                pltpu.VMEM(cot_both, BF16),
                pltpu.VMEM((rows, cols), F32),
                pltpu.VMEM((n, rows, cols), BF16),
                pltpu.VMEM((tokens, cols), BF16),
                pltpu.VMEM((2 * tokens, hq), BF16),
                pltpu.VMEM((tokens, hq), BF16),
                pltpu.VMEM((tokens, cols), F32),
                pltpu.VMEM((n_tp, n, tokens, rows), BF16),
                pltpu.VMEM((chunks, nz, rows, part), F32),
                pltpu.VMEM((chunks, nz, half, part), F32),
                pltpu.VMEM((chunks, nz, half, part), BF16),
                pltpu.VMEM((chunks, nz, half, part), BF16),
                pltpu.VMEM((chunks, nz, rows + half, part), BF16),
                pltpu.VMEM((2, chunks, nz, rows + half, part), BF16),
                pltpu.VMEM((chunks, half, part), BF16),
                pltpu.VMEM((chunks, half, part), BF16),
                pltpu.VMEM((chunks, rows, part), BF16),
                pltpu.VMEM((chunks, rows, part), BF16),
                dma((7,)),
                dma((4, n, 3)),
                dma((n, 4)),
                dma,
                dma,
                dma((n_tp,)),
                dma((n_tp,)),
                dma((chunks,)),
                dma((chunks,)),
                dma((chunks, nz)),
                dma((chunks, nz)),
                dma((chunks, nz)),
                dma((2, chunks, nz)),
                dma((chunks,)),
                dma((chunks,)),
                dma((chunks,)),
                dma((chunks,)),
                dma((n_tp, n)),
                dma((n_tp, n)),
            ],
            compiler_params=pltpu.CompilerParams(
                collective_id=0, has_side_effects=True, vmem_limit_bytes=67043328
            ),
        )(gl, ul, ge, ue, cot, w, gin)
        if not whole_lanes:
            late = late.transpose(1, 0, 2).reshape(tokens, width)
        return late, gg, ug, gout

    placed = (
        P(("rep", "fs"), "tp"),
        P(("rep", "fs"), "tp"),
        P(("rep", "fs"), "tp"),
        P(("rep", "fs"), "tp"),
        P(("rep", "fs"), None),
        P("fs", "tp"),
        P("fs", "tp"),
    )
    return jax.shard_map(
        per_device,
        mesh=mesh,
        in_specs=placed,
        out_specs=(
            P(("rep", "fs"), None),
            P(("rep", "fs"), "tp"),
            P(("rep", "fs"), "tp"),
            P("fs", "tp"),
        ),
        check_vma=False,
    )
```

time: 158 us -> 122 us (0.77)
  Pallas kernels: 148 us -> 113 us
    pallas_call x1, Pallas kernels: 148 us -> 113 us  [per_device(): pl.pallas_call(functools.partial(kernel, n, n_tp, chunks, scale), out_sha...]
where the time goes in v1:
time: 122 us
  Pallas kernels  113 us (93%)
  local copies, waits for them, and re-layouts  8.3 us (7%)
    pallas_call x1, Pallas kernels, per_device(): pl.pallas_call(functools.partial(kernel, n, n_tp, chunks, scale), out_sha...  113 us
    unnamed x10, local copies, waits for them, and re-layouts  8.3 us

profile of v1, /device:TPU:0, one launch (start us, length us, event | category | flops | bytes accessed | tf_op | source)
XLA Modules:
  0.0 122.3 jit_solution(796684421327297470)
XLA Ops:
  0.6 113.3 %shard_map.102 = (bf16[384,2048]{1,0:T(8,128)(2,1)}, bf16[384,2048]{1,0:T(8,128)(2,1)}, bf16[384,2048]{1,0:T(8,128)(2,1)}, f32[256,2048]{1,0:T(8,128)}) custom-call(bf16[384,2048]{1,0:T(8,128)(2,1)} %gl_h.1, bf16[384,2048]{1,0:T(8,128)(2,1)} %ul_h.1, bf16[384,2048]{1,0:T(8,128)(2,1)} %ge_h.1, bf16[384,2048]{1,0:T(8,128)(2,1)} %ue_h.1, ...), custom_call_target="tpu_custom_call" | custom-call | tf_op jit(solution)/shard_map/pallas_call | solution.py:544
  114.0 0.0 copy-start.2
  114.0 2.8 %copy.15 = bf16[384,2048]{1,0:T(8,128)(2,1)} copy(bf16[384,2048]{1,0:T(8,128)(2,1)} %get-tuple-element.8) | data formatting | bytes 3145728
  116.8 0.0 copy-done.2
  116.8 0.0 copy-start.1
  116.8 1.1 copy.16
  118.0 0.8 copy-done.1
  118.8 0.0 copy-start
  118.8 1.1 copy.17
  120.0 1.0 copy-done
  121.0 1.3 %copy.18 = f32[256,2048]{1,0:T(8,128)} copy(f32[256,2048]{1,0:T(8,128)S(1)} %copy-done) | data formatting | bytes 4194304
Async XLA Ops:
  114.0 2.9 %copy-start.2 = (bf16[384,2048]{1,0:T(8,128)(2,1)S(1)}, bf16[384,2048]{1,0:T(8,128)(2,1)}, u32[]{:S(2)}) copy-start(bf16[384,2048]{1,0:T(8,128)(2,1)} %get-tuple-element.9) | copy-start | bytes 4718596
  116.8 2.0 %copy-start.1 = (bf16[384,2048]{1,0:T(8,128)(2,1)S(1)}, bf16[384,2048]{1,0:T(8,128)(2,1)}, u32[]{:S(2)}) copy-start(bf16[384,2048]{1,0:T(8,128)(2,1)} %get-tuple-element.10) | copy-start | bytes 4718596
  118.8 2.2 %copy-start = (f32[256,2048]{1,0:T(8,128)S(1)}, f32[256,2048]{1,0:T(8,128)}, u32[]{:S(2)}) copy-start(f32[256,2048]{1,0:T(8,128)} %get-tuple-element.11) | copy-start | bytes 6291460

commit v2 on v1

--- a/solution.py
+++ b/solution.py
@@ -12,9 +12,16 @@
 F32 = jnp.float32
 BF16 = jnp.bfloat16
 RIGHT, LEFT, ACROSS, OTHER = 0, 1, 2, 3
+LIMIT = 56 << 20
 LAG = 3
 USE_LAG = 6
-SUM_LAG = 6
+START = 3
+RATE = 1
+CHUNKS = 2
+LEAD = 1
+AHEAD = 2
+SETTLE = 0
+DEFER = 4
 TILE = 16
 
 
@@ -202,13 +209,20 @@
                 def _():
                     piece(way, shard, q).start()
 
-                @pl.when(p < 2)
+                @pl.when((p == 0) | ((p == 1) & (hop > 1)))
                 def _():
                     piece(ACROSS, shard, q).start()
 
                 @pl.when(p == 0)
                 def _():
                     piece(OTHER, shard, q).start()
+
+    def deferred():
+        for source in (z - 1, z + 1):
+
+            @pl.when((source >= 0) & (source < nz))
+            def _():
+                piece(ACROSS, 2 * source + y, 1).start()
 
     def gather_across(k):
         hop = lax.div(k, 4) + 1
@@ -267,19 +281,19 @@
             device_id=target(ACROSS), device_id_type=MESH,
         )
 
-    def z_copy(way, c, to):
-        return pltpu.make_async_remote_copy(
-            src_ref=zs.at[c, to], dst_ref=zr.at[way, c, to],
-            send_sem=z_s.at[c, to], recv_sem=z_r.at[way, c, to],
-            device_id=target(way), device_id_type=MESH,
-        )
-
-    def z_arrived(way, c, to):
-        pltpu.make_async_remote_copy(
-            src_ref=zs.at[c, to], dst_ref=zr.at[way, c, to],
-            send_sem=z_s.at[c, to], recv_sem=z_r.at[way, c, to],
-            device_id=target(OTHER), device_id_type=MESH,
-        ).wait_recv()
+    bulk = pl.ds(0, rows)
+    rest = pl.ds(rows, half)
+
+    def z_copy(way, c, to, stage, towards=None):
+        span = (bulk, rest)[stage]
+        return pltpu.make_async_remote_copy(
+            src_ref=zs.at[c, to, span, :], dst_ref=zr.at[way, c, to, span, :],
+            send_sem=z_s.at[stage, c, to], recv_sem=z_r.at[2 * way + stage, c, to],
+            device_id=target(way if towards is None else towards), device_id_type=MESH,
+        )
+
+    def z_arrived(way, c, to, stage):
+        z_copy(way, c, to, stage, OTHER).wait_recv()
 
     def yf_copy(c):
         return pltpu.make_async_remote_copy(
@@ -287,9 +301,10 @@
             device_id=target(ACROSS), device_id_type=MESH,
         )
 
-    def x_copy(c):
-        return pltpu.make_async_remote_copy(
-            src_ref=xs.at[c], dst_ref=xr.at[c], send_sem=x_s.at[c], recv_sem=x_r.at[c],
+    def x_copy(c, stage):
+        return pltpu.make_async_remote_copy(
+            src_ref=xs.at[c, stage], dst_ref=xr.at[c, stage],
+            send_sem=x_s.at[stage, c], recv_sem=x_r.at[stage, c],
             device_id={"rep": other}, device_id_type=MESH,
         )
 
@@ -312,13 +327,11 @@
             opp[c, to] = value[half:]
             own[c, to] = term(y)
 
-    top = pl.ds(0, half)
-    mid = pl.ds(half, half)
-    low = pl.ds(rows, half)
+    first, second = pl.ds(0, half), pl.ds(half, half)
 
     def forward(s):
         for way, place in ((RIGHT, z), (LEFT, nz - 1 - z)):
-            at = s + jnp.where(place == 0, 1, 0)
+            at = s + jnp.where(place == 0, LEAD, 0)
             safe = jnp.maximum(at, 0)
             c = lax.div(safe, nz - 1)
             j = lax.rem(safe, nz - 1) - place
@@ -326,82 +339,95 @@
             @pl.when((at >= 0) & (at < chunks * (nz - 1)) & (j >= 0))
             def _():
                 to = nz - 1 - j if way == RIGHT else j
-                y_copy(c, to).wait_recv()
 
                 @pl.when(place == 0)
                 def _():
-                    zs[c, to, top, :] = (own[c, to, top, :] + yr[c, to].astype(F32)).astype(BF16)
-                    zs[c, to, mid, :] = own[c, to, mid, :].astype(BF16)
-                    zs[c, to, low, :] = opp[c, to].astype(BF16)
+                    zs[c, to, first, :] = own[c, to, second, :].astype(BF16)
+                    zs[c, to, second, :] = opp[c, to].astype(BF16)
 
                 @pl.when(place > 0)
                 def _():
-                    z_arrived(way, c, to)
+                    z_arrived(way, c, to, 0)
                     before = zr.at[way, c, to]
-                    zs[c, to, top, :] = (
-                        own[c, to, top, :] + yr[c, to].astype(F32) + before[top, :].astype(F32)
+                    zs[c, to, first, :] = (own[c, to, second, :] + before[first, :].astype(F32)).astype(BF16)
+                    zs[c, to, second, :] = (opp[c, to] + before[second, :].astype(F32)).astype(BF16)
+
+                z_copy(way, c, to, 0).start()
+                y_copy(c, to).wait_recv()
+
+                @pl.when(place == 0)
+                def _():
+                    zs[c, to, rest, :] = (own[c, to, first, :] + yr[c, to].astype(F32)).astype(BF16)
+
+                @pl.when(place > 0)
+                def _():
+                    z_arrived(way, c, to, 1)
+                    zs[c, to, rest, :] = (
+                        own[c, to, first, :] + yr[c, to].astype(F32) + zr[way, c, to, rest, :].astype(F32)
                     ).astype(BF16)
-                    zs[c, to, mid, :] = (own[c, to, mid, :] + before[mid, :].astype(F32)).astype(BF16)
-                    zs[c, to, low, :] = (opp[c, to] + before[low, :].astype(F32)).astype(BF16)
-
-                z_copy(way, c, to).start()
+
+                z_copy(way, c, to, 1).start()
+
+    sides = ((RIGHT, z > 0), (LEFT, z < nz - 1))
 
     def finish_line(c):
-        y_copy(c, z).wait_recv()
-        own[c, z, top, :] += yr[c, z].astype(F32)
-        for way, there in ((RIGHT, z > 0), (LEFT, z < nz - 1)):
+        for way, there in sides:
 
             @pl.when(there)
             def _():
-                z_arrived(way, c, z)
+                z_arrived(way, c, z, 0)
                 before = zr.at[way, c, z]
-                opp[c, z] += before[low, :].astype(F32)
-                own[c, z] += before[pl.ds(0, rows), :].astype(F32)
+                opp[c, z] += before[second, :].astype(F32)
+                own[c, z, second, :] += before[first, :].astype(F32)
 
         yfs[c] = opp[c, z].astype(BF16)
         yf_copy(c).start()
+        y_copy(c, z).wait_recv()
+        own[c, z, first, :] += yr[c, z].astype(F32)
+        for way, there in sides:
+
+            @pl.when(there)
+            def _():
+                z_arrived(way, c, z, 1)
+                own[c, z, first, :] += zr[way, c, z, rest, :].astype(F32)
+
+        xs[c, 0] = own[c, z, first, :].astype(BF16)
+        x_copy(c, 0).start()
 
     def finish_pair(c):
         yf_copy(c).wait_recv()
-        own[c, z, mid, :] += yfr[c].astype(F32)
-        xs[c] = own[c, z].astype(BF16)
-        x_copy(c).start()
+        own[c, z, second, :] += yfr[c].astype(F32)
+        xs[c, 1] = own[c, z, second, :].astype(BF16)
+        x_copy(c, 1).start()
         lanes = pl.ds(pl.multiple_of(rep * hq + c * width, 128), width)
         gout[:, lanes] = gin[:, lanes] + own[c, z] * scale
 
     def finish_cross(c):
-        x_copy(c).wait_recv()
         lanes = pl.ds(pl.multiple_of(other * hq + c * width, 128), width)
-        gout[:, lanes] = gin[:, lanes] + xr[c].astype(F32) * scale
+        for stage, span in ((0, first), (1, second)):
+            x_copy(c, stage).wait_recv()
+            gout[span, lanes] = gin[span, lanes] + xr[c, stage].astype(F32) * scale
 
     def reduce_step(s):
-        safe = jnp.maximum(s, 0)
-        c = lax.div(safe, nz - 1)
-        t = lax.rem(safe, nz - 1)
-        ahead = jnp.where(s == -2, 0, c + 1)
-
-        @pl.when(((s == -2) | ((s >= 0) & (t == 0))) & (ahead < chunks))
-        def _():
-            contribute(ahead)
-
+        def when_due(offset, ready, act):
+            at = s - offset
+            safe = jnp.maximum(at, 0)
+            c = lax.div(safe, nz - 1) + ready
+
+            @pl.when((at >= 0) & (lax.rem(safe, nz - 1) == 0) & (c >= 0) & (c < chunks))
+            def _():
+                act(c)
+
+        when_due(-LEAD - AHEAD, 0, contribute)
         forward(s)
-        done = c - 1
-
-        @pl.when((t == 0) & (done >= 0) & (done < chunks))
-        def _():
-            finish_line(done)
-
-        @pl.when((t == 1) & (done >= 0) & (done < chunks))
-        def _():
-            finish_pair(done)
-
-        @pl.when((t == 2) & (done >= 0) & (done < chunks))
-        def _():
-            finish_cross(done)
+        when_due(SETTLE, -1, finish_line)
+        when_due(SETTLE + 1, -1, finish_pair)
+        when_due(SETTLE + 2, -1, finish_cross)
 
     gather_ticks = 4 * (nz - 1)
     use_ticks = max(2 * n - 3, n + USE_LAG)
-    sum_ticks = SUM_LAG + chunks * (nz - 1) + 2
+    sum_steps = chunks * (nz - 1) + LEAD + AHEAD + SETTLE + 2
+    sum_ticks = START + -(-sum_steps // RATE)
 
     def used(k):
         return jnp.clip(jnp.minimum(lax.div(k + 2, 2), k - USE_LAG) + 1, 1, n)
@@ -422,21 +448,28 @@
             piece_arrived(beyond, 0)
             piece(OTHER, beyond, 0).start()
 
-        @pl.when(k == SUM_LAG - 3)
+        @pl.when(k == START - 1)
         def _():
             cot_cross().wait_recv()
             for j in range(1, n_tp):
                 cot_share(j, tp).start()
 
-        @pl.when(k == SUM_LAG - 2)
+        @pl.when(k == START)
         def _():
             for j in range(1, n_tp):
                 cot_share(j, lax.rem(tp + n_tp - j, n_tp)).wait_recv()
             loads(6).wait()
 
-        @pl.when((k >= SUM_LAG - 2) & (k < sum_ticks))
-        def _():
-            reduce_step(k - SUM_LAG)
+        for r in range(RATE):
+            step = (k - START) * RATE + r
+
+            @pl.when((step >= 0) & (step < sum_steps))
+            def _():
+                reduce_step(step - LEAD - AHEAD)
+
+        @pl.when(k == DEFER)
+        def _():
+            deferred()
 
         lax.fori_loop(jnp.where(k == 0, 0, used(k - 1)), used(k), use, 0)
         return carry
@@ -466,7 +499,7 @@
         else:
             late[shard] = total.astype(BF16)
 
-    reduce_step(jnp.int32(chunks * (nz - 1) + 2))
+    reduce_step(jnp.int32(chunks * (nz - 1) + SETTLE + 2))
 
     cot_cross().wait_send()
     for k in range(1, n_tp):
@@ -509,17 +542,32 @@
 
             @pl.when(at > z)
             def _():
-                z_copy(RIGHT, c, at).wait_send()
+                z_copy(RIGHT, c, at, 0).wait_send()
+                z_copy(RIGHT, c, at, 1).wait_send()
 
             @pl.when(at < z)
             def _():
-                z_copy(LEFT, c, at).wait_send()
+                z_copy(LEFT, c, at, 0).wait_send()
+                z_copy(LEFT, c, at, 1).wait_send()
 
     @pl.loop(0, chunks)
     def _(c):
         he_cross(c).wait_send()
         yf_copy(c).wait_send()
-        x_copy(c).wait_send()
+        x_copy(c, 0).wait_send()
+        x_copy(c, 1).wait_send()
+
+
+def deliver(*refs):
+    count = 4
+    sems = refs[-1]
+    copies = [
+        pltpu.make_async_copy(refs[i], refs[count + i], sems.at[i]) for i in range(count)
+    ]
+    for copy in copies:
+        copy.start()
+    for copy in copies:
+        copy.wait()
 
 
 def solution(mesh):
@@ -531,7 +579,7 @@
         rows, width = w.shape[0], cotangent.shape[1]
         assert rows % 64 == 0 and cols % 256 == 0
         nz, hq, half = n // 2, cols // 2, rows // 2
-        chunks = 2
+        chunks = min(CHUNKS, hq // 128)
         scale = 1.0 / math.sqrt(tokens * n_rep * n)
         whole_lanes = rows % 128 == 0
         cot = cotangent
@@ -544,10 +592,10 @@
         late, gg, ug, gout = pl.pallas_call(
             functools.partial(kernel, n, n_tp, chunks, scale),
             out_shape=(
-                jax.ShapeDtypeStruct(cot.shape, BF16),
-                jax.ShapeDtypeStruct((tokens, cols), BF16),
-                jax.ShapeDtypeStruct((tokens, cols), BF16),
-                jax.ShapeDtypeStruct((rows, cols), F32),
+                pltpu.VMEM(cot.shape, BF16),
+                pltpu.VMEM((tokens, cols), BF16),
+                pltpu.VMEM((tokens, cols), BF16),
+                pltpu.VMEM((rows, cols), F32),
             ),
             in_specs=[pl.BlockSpec(memory_space=pl.ANY)] * 7,
             out_specs=(vmem,) * 4,
@@ -572,8 +620,8 @@
                 pltpu.VMEM((2, chunks, nz, rows + half, part), BF16),
                 pltpu.VMEM((chunks, half, part), BF16),
                 pltpu.VMEM((chunks, half, part), BF16),
-                pltpu.VMEM((chunks, rows, part), BF16),
-                pltpu.VMEM((chunks, rows, part), BF16),
+                pltpu.VMEM((chunks, 2, half, part), BF16),
+                pltpu.VMEM((chunks, 2, half, part), BF16),
                 dma((7,)),
                 dma((4, n, 3)),
                 dma((n, 4)),
@@ -585,19 +633,27 @@
                 dma((chunks,)),
                 dma((chunks, nz)),
                 dma((chunks, nz)),
-                dma((chunks, nz)),
                 dma((2, chunks, nz)),
+                dma((4, chunks, nz)),
                 dma((chunks,)),
                 dma((chunks,)),
-                dma((chunks,)),
-                dma((chunks,)),
+                dma((2, chunks)),
+                dma((2, chunks)),
                 dma((n_tp, n)),
                 dma((n_tp, n)),
             ],
             compiler_params=pltpu.CompilerParams(
-                collective_id=0, has_side_effects=True, vmem_limit_bytes=67043328
+                collective_id=0, has_side_effects=True, vmem_limit_bytes=LIMIT
             ),
         )(gl, ul, ge, ue, cot, w, gin)
+        late, gg, ug, gout = pl.pallas_call(
+            deliver,
+            out_shape=tuple(jax.ShapeDtypeStruct(a.shape, a.dtype) for a in (late, gg, ug, gout)),
+            in_specs=[pl.BlockSpec(memory_space=pl.ANY)] * 4,
+            out_specs=(pl.BlockSpec(memory_space=pl.ANY),) * 4,
+            scratch_shapes=[dma((4,))],
+            compiler_params=pltpu.CompilerParams(vmem_limit_bytes=1 << 20),
+        )(late, gg, ug, gout)
         if not whole_lanes:
             late = late.transpose(1, 0, 2).reshape(tokens, width)
         return late, gg, ug, gout

time: 122 us -> 107 us (0.88)
  local copies, waits for them, and re-layouts: 8.3 us -> 0 us
  Pallas kernels: 113 us -> 107 us
    pallas_call x1, Pallas kernels: 113 us -> 104 us  [per_device(): pl.pallas_call(functools.partial(kernel, n, n_tp, chunks, scale), out_sha...]
    unnamed x10 -> x0, local copies, waits for them, and re-layouts: 8.3 us -> none
    pallas_call x0 -> x1, Pallas kernels: none -> 2.91 us  [per_device(): pl.pallas_call(deliver, out_shape=tuple((jax.ShapeDtypeStruct(a.shape, a....]
where the time goes in v2:
time: 107 us
  Pallas kernels  107 us (100%)
    pallas_call x1, Pallas kernels, per_device(): pl.pallas_call(functools.partial(kernel, n, n_tp, chunks, scale), out_sha...  104 us
    pallas_call x1, Pallas kernels, per_device(): pl.pallas_call(deliver, out_shape=tuple((jax.ShapeDtypeStruct(a.shape, a....  2.91 us

profile of v2, /device:TPU:0, one launch (start us, length us, event | category | flops | bytes accessed | tf_op | source)
XLA Modules:
  0.0 107.2 jit_solution(3513290824473023559)
XLA Ops:
  0.6 103.6 %shard_map.102 = (bf16[384,2048]{1,0:T(8,128)(2,1)S(1)}, bf16[384,2048]{1,0:T(8,128)(2,1)S(1)}, bf16[384,2048]{1,0:T(8,128)(2,1)S(1)}, f32[256,2048]{1,0:T(8,128)S(1)}) custom-call(bf16[384,2048]{1,0:T(8,128)(2,1)} %gl_h.1, bf16[384,2048]{1,0:T(8,128)(2,1)} %ul_h.1, bf16[384,2048]{1,0:T(8,128)(2,1)} %ge_h.1, bf16[384,2048]{1,0:T(8,128)(2,1)} %ue_h.1, ...), custom_call_target="tpu_custom_call" | custom-call | tf_op jit(solution)/shard_map/pallas_call | solution.py:592
  104.3 2.9 %shard_map.103 = (bf16[384,2048]{1,0:T(8,128)(2,1)}, bf16[384,2048]{1,0:T(8,128)(2,1)}, bf16[384,2048]{1,0:T(8,128)(2,1)}, f32[256,2048]{1,0:T(8,128)}) custom-call(bf16[384,2048]{1,0:T(8,128)(2,1)S(1)} %get-tuple-element.8.refs_0_, bf16[384,2048]{1,0:T(8,128)(2,1)S(1)} %get-tuple-element.9.refs_1_, bf16[384,2048]{1,0:T(8,128)(2,1)S(1)} %get-tuple-element.10.refs_2_, ...), custom_call_target="tpu_custom_call" | custom-call | tf_op jit(solution)/shard_map/pallas_call | solution.py:649

commit v3 on v2

--- a/solution.py
+++ b/solution.py
@@ -13,15 +13,24 @@
 BF16 = jnp.bfloat16
 RIGHT, LEFT, ACROSS, OTHER = 0, 1, 2, 3
 LIMIT = 56 << 20
-LAG = 3
-USE_LAG = 6
-START = 3
-RATE = 1
 CHUNKS = 2
-LEAD = 1
-AHEAD = 2
-SETTLE = 0
-DEFER = 4
+LEAD = 2
+AHEAD = (1, 3)
+SETTLE = (1, 1)
+START = (2, 1)
+LAG = (2, 5)
+USE_LAG = (5, 7)
+Y0 = 0
+Y1 = 1
+Y1H = 1
+F1 = (1, 0)
+RSFIRST = 1
+YI = 1
+HOLD = 1
+FP = (2, 2)
+FC = (2, 2)
+P1 = 5
+H0 = 7
 TILE = 16
 
 
@@ -35,7 +44,9 @@
     tokens, cols = gl.shape
     rows = wf.shape[1]
     quarter = rows // 4
-    half = rows // 2
+    third = max(rows * P1 // 256, 1) * 16
+    head = max(rows * H0 // 256, 1) * 16
+    tail = rows - head
     nz = n // 2
     hq = cols // 2
     width = hq // chunks
@@ -46,6 +57,15 @@
     y = lax.rem(me, 2)
     other = 1 - rep
     flat = len(cot.shape) == 2
+    end = (z == 0) | (z == nz - 1)
+
+    def pick(pair):
+        return pair[0] if pair[0] == pair[1] else jnp.where(end, pair[0], pair[1])
+
+    lead, ahead, settle = LEAD, pick(AHEAD), pick(SETTLE)
+    begin, lag, use_lag, split = pick(START), pick(LAG), pick(USE_LAG), pick(F1)
+    pair_due = settle + pick(FP)
+    cross_due = pair_due + pick(FC)
 
     def cot_tokens(ref, start, size):
         return ref.at[pl.ds(start, size), :] if flat else ref.at[:, pl.ds(start, size), :]
@@ -57,7 +77,7 @@
         )
         return pltpu.make_async_copy(pairs[i][0], pairs[i][1], ld.at[i])
 
-    for i in range(7):
+    for i in range(4):
         loads(i).start()
 
     barrier = pltpu.get_barrier_semaphore()
@@ -87,7 +107,9 @@
         return {"rep": other}
 
     def piece_rows(p):
-        return pl.ds(pl.multiple_of((p + rep * (3 - 2 * p)) * quarter, 16), quarter)
+        size = (quarter, third, rows - 2 * quarter - third, quarter)[p]
+        start = (0, quarter, quarter + third, rows - quarter)[p]
+        return pl.ds(pl.multiple_of(start + rep * (rows - 2 * start - size), 16), size)
 
     def piece(way, shard, p):
         spot = wf.at[shard, piece_rows(p), :]
@@ -106,7 +128,8 @@
 
     loads(0).wait()
     for p in range(3):
-        piece(ACROSS, me, (2, 0, 1)[p]).start()
+        if p < 2 or YI < 0:
+            piece(ACROSS, me, (2, 0, 1)[p]).start()
 
         @pl.when(z < nz - 1)
         def _():
@@ -115,76 +138,6 @@
         @pl.when(z > 0)
         def _():
             piece(LEFT, me, p).start()
-
-    lot = tokens // n_tp
-
-    def cot_cross():
-        return pltpu.make_async_remote_copy(
-            src_ref=cot_tokens(cot, pl.multiple_of(tp * lot, 16), lot),
-            dst_ref=cot_tokens(cot, pl.multiple_of(tokens + tp * lot, 16), lot),
-            send_sem=cx_s, recv_sem=cx_r, device_id={"rep": other}, device_id_type=MESH,
-        )
-
-    def cot_share(k, sender):
-        spot = cot_tokens(cot, pl.multiple_of(tokens + sender * lot, 16), lot)
-        return pltpu.make_async_remote_copy(
-            src_ref=spot, dst_ref=spot, send_sem=ct_s.at[k], recv_sem=ct_r.at[k],
-            device_id={"tp": lax.rem(tp + k, n_tp)}, device_id_type=MESH,
-        )
-
-    loads(1).wait()
-    cot_cross().start()
-
-    def columns(c):
-        return pl.ds(pl.multiple_of(c * width, 128), width)
-
-    def he_cross(c):
-        return pltpu.make_async_remote_copy(
-            src_ref=he_out.at[:, columns(c)], dst_ref=he.at[pl.ds(tokens, tokens), columns(c)],
-            send_sem=he_s.at[c], recv_sem=he_r.at[c], device_id={"rep": other}, device_id_type=MESH,
-        )
-
-    def tile_at(i):
-        return pl.ds(pl.multiple_of(i * TILE, TILE), TILE)
-
-    def gated(gate_ref, up_ref, span, lanes):
-        gate = gate_ref[span, lanes].astype(F32)
-        return (gate * (1.0 / (1.0 + jnp.exp(-gate))) * up_ref[span, lanes].astype(F32)).astype(BF16)
-
-    mine_lanes = pl.ds(pl.multiple_of(rep * hq, 128), hq)
-    theirs_lanes = pl.ds(pl.multiple_of(other * hq, 128), hq)
-    loads(2).wait()
-    loads(3).wait()
-
-    @pl.loop(0, tokens // TILE)
-    def _(i):
-        he_out[tile_at(i), :] = gated(ge, ue, tile_at(i), theirs_lanes)
-
-    for c in range(chunks):
-        he_cross(c).start()
-
-    @pl.loop(0, tokens // TILE)
-    def _(i):
-        he[tile_at(i), :] = gated(ge, ue, tile_at(i), mine_lanes)
-
-    beyond = 2 * z + 1 - y
-    piece_arrived(beyond, 2)
-
-    @pl.when(z < nz - 1)
-    def _():
-        piece(RIGHT, beyond, 2).start()
-
-    @pl.when(z > 0)
-    def _():
-        piece(LEFT, beyond, 2).start()
-
-    loads(4).wait()
-    loads(5).wait()
-
-    @pl.loop(0, tokens // TILE)
-    def _(i):
-        hl[tile_at(i), :] = gated(gl, ul, tile_at(i), slice(None))
-        hg[tile_at(i), :] = jnp.zeros((TILE, cols), F32)
 
     def nearest(m):
         low = jnp.minimum(z, nz - 1 - z)
@@ -193,36 +146,126 @@
         down = jnp.where(paired, lax.rem(m, 2) == 1, 2 * z > nz - 1)
         return jnp.where(down, z - step, z + step)
 
+    for i in range(4, 7):
+        loads(i).start()
+
+    lot = tokens // n_tp
+
+    def cot_piece(start, to):
+        span = pl.ds(pl.multiple_of(start, 16), lot)
+        if flat:
+            return cot.at[span, pl.ds(pl.multiple_of(2 * to * rows, 2 * rows), 2 * rows)]
+        return cot.at[pl.ds(2 * to, 2), span, :]
+
+    def cot_cross(to):
+        return pltpu.make_async_remote_copy(
+            src_ref=cot_piece(tp * lot, to), dst_ref=cot_piece(tokens + tp * lot, to),
+            send_sem=cx_s.at[to], recv_sem=cx_r.at[to],
+            device_id={"rep": other}, device_id_type=MESH,
+        )
+
+    def cot_share(k, sender, to):
+        spot = cot_piece(tokens + sender * lot, to)
+        return pltpu.make_async_remote_copy(
+            src_ref=spot, dst_ref=spot, send_sem=ct_s.at[k, to], recv_sem=ct_r.at[k, to],
+            device_id={"tp": lax.rem(tp + k, n_tp)}, device_id_type=MESH,
+        )
+
+    loads(1).wait()
+    cot_cross(nearest(nz - 1)).start()
+
+    def columns(c):
+        return pl.ds(pl.multiple_of(c * width, 128), width)
+
+    def he_cross(c):
+        return pltpu.make_async_remote_copy(
+            src_ref=he_out.at[:, columns(c)], dst_ref=he.at[pl.ds(tokens, tokens), columns(c)],
+            send_sem=he_s.at[c], recv_sem=he_r.at[c], device_id={"rep": other}, device_id_type=MESH,
+        )
+
+    def tile_at(i):
+        return pl.ds(pl.multiple_of(i * TILE, TILE), TILE)
+
+    def gated(gate_ref, up_ref, span, lanes):
+        gate = gate_ref[span, lanes].astype(F32)
+        return (gate * (1.0 / (1.0 + jnp.exp(-gate))) * up_ref[span, lanes].astype(F32)).astype(BF16)
+
+    mine_lanes = pl.ds(pl.multiple_of(rep * hq, 128), hq)
+    theirs_lanes = pl.ds(pl.multiple_of(other * hq, 128), hq)
+    loads(2).wait()
+    loads(3).wait()
+
+    @pl.loop(0, tokens // TILE)
+    def _(i):
+        he_out[tile_at(i), :] = gated(ge, ue, tile_at(i), theirs_lanes)
+
+    he_cross(0).start()
+
+    @pl.loop(1, nz)
+    def _(m):
+        cot_cross(nearest(nz - 1 - m)).start()
+
+    for c in range(1, chunks):
+        he_cross(c).start()
+
+    @pl.loop(0, tokens // TILE)
+    def _(i):
+        he[tile_at(i), :] = gated(ge, ue, tile_at(i), mine_lanes)
+
+    beyond = 2 * z + 1 - y
+    piece_arrived(beyond, 2)
+
+    @pl.when(z < nz - 1)
+    def _():
+        piece(RIGHT, beyond, 2).start()
+
+    @pl.when(z > 0)
+    def _():
+        piece(LEFT, beyond, 2).start()
+
+    loads(4).wait()
+    loads(5).wait()
+
+    @pl.loop(0, tokens // TILE)
+    def _(i):
+        hl[tile_at(i), :] = gated(gl, ul, tile_at(i), slice(None))
+        hg[tile_at(i), :] = jnp.zeros((TILE, cols), F32)
+
+    def onward(k, arrive, pass_on):
+        hop = lax.div(k, 4) + 1
+        for p in range(4):
+            line = 1 - y if p == 3 else y
+            q = 2 if p == 3 else p
+            for source, step, way in ((z - hop, 1, RIGHT), (z + hop, -1, LEFT)):
+                shard = 2 * source + line
+
+                @pl.when((lax.rem(k, 4) == p) & (source >= 0) & (source < nz))
+                def _():
+                    if arrive:
+                        piece_arrived(shard, q)
+
+                    @pl.when((z + step >= 0) & (z + step < nz) & pass_on(hop))
+                    def _():
+                        piece(way, shard, q).start()
+
+                    if arrive and p == 0:
+                        if Y0 == 0:
+                            piece(ACROSS, shard, 0).start()
+                        piece(OTHER, shard, 0).start()
+
     def gather(k):
+        onward(k, True, lambda hop: (hop < 2) | (HOLD == 0))
+
+    def held(k):
+        onward(k, False, lambda hop: hop >= 2)
+
+    def across(k, p):
         hop = lax.div(k, 4) + 1
-        p = lax.rem(k, 4)
-        line = jnp.where(p == 3, 1 - y, y)
-        q = jnp.where(p == 3, 2, p)
-        for source, onward, way in ((z - hop, z + 1, RIGHT), (z + hop, z - 1, LEFT)):
+        for source in (z - hop, z + hop):
 
             @pl.when((source >= 0) & (source < nz))
             def _():
-                shard = 2 * source + line
-                piece_arrived(shard, q)
-
-                @pl.when((onward >= 0) & (onward < nz))
-                def _():
-                    piece(way, shard, q).start()
-
-                @pl.when((p == 0) | ((p == 1) & (hop > 1)))
-                def _():
-                    piece(ACROSS, shard, q).start()
-
-                @pl.when(p == 0)
-                def _():
-                    piece(OTHER, shard, q).start()
-
-    def deferred():
-        for source in (z - 1, z + 1):
-
-            @pl.when((source >= 0) & (source < nz))
-            def _():
-                piece(ACROSS, 2 * source + y, 1).start()
+                piece(ACROSS, 2 * source + y, p).start()
 
     def gather_across(k):
         hop = lax.div(k, 4) + 1
@@ -281,8 +324,10 @@
             device_id=target(ACROSS), device_id_type=MESH,
         )
 
-    bulk = pl.ds(0, rows)
-    rest = pl.ds(rows, half)
+    first, second = halves = pl.ds(0, head), pl.ds(head, tail)
+    mine, cross = pl.ds(0, tail), pl.ds(tail, tail)
+    bulk = pl.ds(0, 2 * tail)
+    rest = pl.ds(2 * tail, head)
 
     def z_copy(way, c, to, stage, towards=None):
         span = (bulk, rest)[stage]
@@ -303,31 +348,41 @@
 
     def x_copy(c, stage):
         return pltpu.make_async_remote_copy(
-            src_ref=xs.at[c, stage], dst_ref=xr.at[c, stage],
+            src_ref=xs.at[c, halves[stage], :], dst_ref=xr.at[c, halves[stage], :],
             send_sem=x_s.at[stage, c], recv_sem=x_r.at[stage, c],
             device_id={"rep": other}, device_id_type=MESH,
         )
 
-    def contribute(c):
-        he_cross(c).wait_recv()
-
-        @pl.loop(0, nz)
-        def _(m):
-            to = nearest(nz - 1 - m)
-
-            def term(line):
-                return lax.dot_general(
-                    cot_block(0, 2 * tokens, 2 * to + line), he[:, columns(c)],
-                    (((0,), (0,)), ((), ())), preferred_element_type=F32,
-                )
-
-            value = term(1 - y)
-            ys[c, to] = value[:half].astype(BF16)
-            y_copy(c, to).start()
-            opp[c, to] = value[half:]
-            own[c, to] = term(y)
-
-    first, second = pl.ds(0, half), pl.ds(half, half)
+    def contribute(c, m):
+        to = nearest(nz - 1 - m)
+
+        @pl.when(c == 0)
+        def _():
+            cot_cross(to).wait_recv()
+            for k in range(1, n_tp):
+                cot_share(k, tp, to).start()
+
+        @pl.when(m == 0)
+        def _():
+            he_cross(c).wait_recv()
+
+        @pl.when(c == 0)
+        def _():
+            for k in range(1, n_tp):
+                cot_share(k, lax.rem(tp + n_tp - k, n_tp), to).wait_recv()
+
+        def term(line):
+            return lax.dot_general(
+                cot_block(0, 2 * tokens, 2 * to + line), he[:, columns(c)],
+                (((0,), (0,)), ((), ())), preferred_element_type=F32,
+            )
+
+        value = term(1 - y)
+        ys[c, to] = value[:head].astype(BF16)
+        y_copy(c, to).start()
+        opp[c, to] = value[head:]
+        own[c, to] = term(y)
+
 
     def forward(s):
         for way, place in ((RIGHT, z), (LEFT, nz - 1 - z)):
@@ -342,17 +397,28 @@
 
                 @pl.when(place == 0)
                 def _():
-                    zs[c, to, first, :] = own[c, to, second, :].astype(BF16)
-                    zs[c, to, second, :] = opp[c, to].astype(BF16)
+                    zs[c, to, mine, :] = own[c, to, second, :].astype(BF16)
+                    zs[c, to, cross, :] = opp[c, to].astype(BF16)
 
                 @pl.when(place > 0)
                 def _():
                     z_arrived(way, c, to, 0)
                     before = zr.at[way, c, to]
-                    zs[c, to, first, :] = (own[c, to, second, :] + before[first, :].astype(F32)).astype(BF16)
-                    zs[c, to, second, :] = (opp[c, to] + before[second, :].astype(F32)).astype(BF16)
+                    zs[c, to, mine, :] = (own[c, to, second, :] + before[mine, :].astype(F32)).astype(BF16)
+                    zs[c, to, cross, :] = (opp[c, to] + before[cross, :].astype(F32)).astype(BF16)
 
                 z_copy(way, c, to, 0).start()
+
+    def forward_rest(s):
+        for way, place in ((RIGHT, z), (LEFT, nz - 1 - z)):
+            at = s + jnp.where(place == 0, LEAD, 0)
+            safe = jnp.maximum(at, 0)
+            c = lax.div(safe, nz - 1)
+            j = lax.rem(safe, nz - 1) - place
+
+            @pl.when((at >= 0) & (at < chunks * (nz - 1)) & (j >= 0))
+            def _():
+                to = nz - 1 - j if way == RIGHT else j
                 y_copy(c, to).wait_recv()
 
                 @pl.when(place == 0)
@@ -377,8 +443,8 @@
             def _():
                 z_arrived(way, c, z, 0)
                 before = zr.at[way, c, z]
-                opp[c, z] += before[second, :].astype(F32)
-                own[c, z, second, :] += before[first, :].astype(F32)
+                opp[c, z] += before[cross, :].astype(F32)
+                own[c, z, second, :] += before[mine, :].astype(F32)
 
         yfs[c] = opp[c, z].astype(BF16)
         yf_copy(c).start()
@@ -391,13 +457,13 @@
                 z_arrived(way, c, z, 1)
                 own[c, z, first, :] += zr[way, c, z, rest, :].astype(F32)
 
-        xs[c, 0] = own[c, z, first, :].astype(BF16)
+        xs[c, first, :] = own[c, z, first, :].astype(BF16)
         x_copy(c, 0).start()
 
     def finish_pair(c):
         yf_copy(c).wait_recv()
         own[c, z, second, :] += yfr[c].astype(F32)
-        xs[c, 1] = own[c, z, second, :].astype(BF16)
+        xs[c, second, :] = own[c, z, second, :].astype(BF16)
         x_copy(c, 1).start()
         lanes = pl.ds(pl.multiple_of(rep * hq + c * width, 128), width)
         gout[:, lanes] = gin[:, lanes] + own[c, z] * scale
@@ -406,7 +472,7 @@
         lanes = pl.ds(pl.multiple_of(other * hq + c * width, 128), width)
         for stage, span in ((0, first), (1, second)):
             x_copy(c, stage).wait_recv()
-            gout[span, lanes] = gin[span, lanes] + xr[c, stage].astype(F32) * scale
+            gout[span, lanes] = gin[span, lanes] + xr[c, span, :].astype(F32) * scale
 
     def reduce_step(s):
         def when_due(offset, ready, act):
@@ -418,59 +484,81 @@
             def _():
                 act(c)
 
-        when_due(-LEAD - AHEAD, 0, contribute)
+        base = s + lead + ahead
+
+        @pl.loop(0, 2)
+        def _(turn):
+            late_turn = 1 - turn
+            c = lax.div(base, nz - 1) - late_turn
+            m = lax.rem(base, nz - 1) + late_turn * (nz - 1)
+
+            @pl.when((m < nz) & (c >= 0) & (c < chunks))
+            def _():
+                contribute(c, m)
+
         forward(s)
-        when_due(SETTLE, -1, finish_line)
-        when_due(SETTLE + 1, -1, finish_pair)
-        when_due(SETTLE + 2, -1, finish_cross)
+        forward_rest(s - split)
+        when_due(settle, -1, finish_line)
+        when_due(pair_due, -1, finish_pair)
+        when_due(cross_due, -1, finish_cross)
 
     gather_ticks = 4 * (nz - 1)
-    use_ticks = max(2 * n - 3, n + USE_LAG)
-    sum_steps = chunks * (nz - 1) + LEAD + AHEAD + SETTLE + 2
-    sum_ticks = START + -(-sum_steps // RATE)
+    use_ticks = max(2 * n - 3, n + max(USE_LAG))
+    last_step = chunks * (nz - 1) + cross_due
+    sum_ticks = max(
+        START[i] + chunks * (nz - 1) + LEAD + AHEAD[i] + SETTLE[i] + FP[i] + FC[i] for i in range(2)
+    )
 
     def used(k):
-        return jnp.clip(jnp.minimum(lax.div(k + 2, 2), k - USE_LAG) + 1, 1, n)
+        return jnp.clip(jnp.minimum(lax.div(k + 2, 2), k - use_lag) + 1, 1, n)
+
+    def reduce_tick(k):
+        step = k - begin - lead - ahead
+
+        @pl.when((k >= begin) & (step < last_step))
+        def _():
+            reduce_step(step)
+
+    def when_gathering(k, act, *more):
+        @pl.when((k >= 0) & (k < gather_ticks) & functools.reduce(jnp.logical_and, more, True))
+        def _():
+            act(k)
 
     def tick(k, carry):
-        @pl.when(k < gather_ticks)
-        def _():
-            gather(k)
-
-        late_k = k - LAG
-
-        @pl.when((late_k >= 0) & (late_k < gather_ticks) & (lax.rem(jnp.maximum(late_k, 0), 4) == 0))
-        def _():
-            gather_across(late_k)
+        if RSFIRST == 1:
+            reduce_tick(k)
+        when_gathering(k, gather)
+        behind = k - lag
+        when_gathering(behind, gather_across, lax.rem(jnp.maximum(behind, 0), 4) == 0)
 
         @pl.when(k == 1)
         def _():
             piece_arrived(beyond, 0)
             piece(OTHER, beyond, 0).start()
 
-        @pl.when(k == START - 1)
-        def _():
-            cot_cross().wait_recv()
-            for j in range(1, n_tp):
-                cot_share(j, tp).start()
-
-        @pl.when(k == START)
-        def _():
-            for j in range(1, n_tp):
-                cot_share(j, lax.rem(tp + n_tp - j, n_tp)).wait_recv()
+        @pl.when(k == max(START))
+        def _():
             loads(6).wait()
 
-        for r in range(RATE):
-            step = (k - START) * RATE + r
-
-            @pl.when((step >= 0) & (step < sum_steps))
-            def _():
-                reduce_step(step - LEAD - AHEAD)
-
-        @pl.when(k == DEFER)
-        def _():
-            deferred()
-
+        if RSFIRST == 0:
+            reduce_tick(k)
+        if Y0 > 0:
+            at = k - Y0
+            when_gathering(at, lambda j: across(j, 0), lax.rem(jnp.maximum(at, 0), 4) == 0)
+        at = k - Y1
+        when_gathering(at, lambda j: across(j, 1), lax.rem(jnp.maximum(at, 0), 4) == 1, (at < 4) | (Y1H == 0))
+        if Y1H:
+            when_gathering(k, lambda j: across(j, 1), lax.rem(k, 4) == 1, k >= 4)
+        if HOLD:
+            when_gathering(k - HOLD, held)
+        if YI >= 0:
+
+            @pl.when(k == YI)
+            def _():
+                piece(ACROSS, me, 1).start()
+
+        if RSFIRST == 2:
+            reduce_tick(k)
         lax.fori_loop(jnp.where(k == 0, 0, used(k - 1)), used(k), use, 0)
         return carry
 
@@ -499,11 +587,8 @@
         else:
             late[shard] = total.astype(BF16)
 
-    reduce_step(jnp.int32(chunks * (nz - 1) + SETTLE + 2))
-
-    cot_cross().wait_send()
-    for k in range(1, n_tp):
-        cot_share(k, tp).wait_send()
+    reduce_step(jnp.int32(last_step))
+
     for p in range(3):
         piece(ACROSS, me, p).wait_send()
 
@@ -525,6 +610,7 @@
             piece(LEFT, crossed, 2).wait_send()
 
         piece(OTHER, crossed, 0).wait_send()
+        cot_cross(at).wait_send()
 
         @pl.when(at != z)
         def _():
@@ -533,6 +619,7 @@
                 piece(ACROSS, same, p).wait_send()
 
         for k in range(1, n_tp):
+            cot_share(k, tp, at).wait_send()
             share(k, same).wait_send()
             share(k, crossed).wait_send()
 
@@ -578,7 +665,9 @@
         tokens, cols = gl.shape
         rows, width = w.shape[0], cotangent.shape[1]
         assert rows % 64 == 0 and cols % 256 == 0
-        nz, hq, half = n // 2, cols // 2, rows // 2
+        nz, hq = n // 2, cols // 2
+        head = max(rows * H0 // 256, 1) * 16
+        tail = rows - head
         chunks = min(CHUNKS, hq // 128)
         scale = 1.0 / math.sqrt(tokens * n_rep * n)
         whole_lanes = rows % 128 == 0
@@ -613,22 +702,22 @@
                 pltpu.VMEM((tokens, cols), F32),
                 pltpu.VMEM((n_tp, n, tokens, rows), BF16),
                 pltpu.VMEM((chunks, nz, rows, part), F32),
-                pltpu.VMEM((chunks, nz, half, part), F32),
-                pltpu.VMEM((chunks, nz, half, part), BF16),
-                pltpu.VMEM((chunks, nz, half, part), BF16),
-                pltpu.VMEM((chunks, nz, rows + half, part), BF16),
-                pltpu.VMEM((2, chunks, nz, rows + half, part), BF16),
-                pltpu.VMEM((chunks, half, part), BF16),
-                pltpu.VMEM((chunks, half, part), BF16),
-                pltpu.VMEM((chunks, 2, half, part), BF16),
-                pltpu.VMEM((chunks, 2, half, part), BF16),
+                pltpu.VMEM((chunks, nz, tail, part), F32),
+                pltpu.VMEM((chunks, nz, head, part), BF16),
+                pltpu.VMEM((chunks, nz, head, part), BF16),
+                pltpu.VMEM((chunks, nz, rows + tail, part), BF16),
+                pltpu.VMEM((2, chunks, nz, rows + tail, part), BF16),
+                pltpu.VMEM((chunks, tail, part), BF16),
+                pltpu.VMEM((chunks, tail, part), BF16),
+                pltpu.VMEM((chunks, rows, part), BF16),
+                pltpu.VMEM((chunks, rows, part), BF16),
                 dma((7,)),
                 dma((4, n, 3)),
                 dma((n, 4)),
-                dma,
-                dma,
-                dma((n_tp,)),
-                dma((n_tp,)),
+                dma((nz,)),
+                dma((nz,)),
+                dma((n_tp, nz)),
+                dma((n_tp, nz)),
                 dma((chunks,)),
                 dma((chunks,)),
                 dma((chunks, nz)),

time: 107 us -> 100 us (0.935)
  Pallas kernels: 107 us -> 99.6 us
    pallas_call x1, Pallas kernels: 104 us -> 96.7 us  [per_device(): pl.pallas_call(functools.partial(kernel, n, n_tp, chunks, scale), out_sha...]
where the time goes in v3:
time: 100 us
  Pallas kernels  99.6 us (100%)
    pallas_call x1, Pallas kernels, per_device(): pl.pallas_call(functools.partial(kernel, n, n_tp, chunks, scale), out_sha...  96.7 us
    pallas_call x1, Pallas kernels, per_device(): pl.pallas_call(deliver, out_shape=tuple((jax.ShapeDtypeStruct(a.shape, a....  2.91 us

profile of v3, /device:TPU:0, one launch (start us, length us, event | category | flops | bytes accessed | tf_op | source)
XLA Modules:
  0.0 100.2 jit_solution(11483896669984060269)
XLA Ops:
  0.6 96.7 %shard_map.102 = (bf16[384,2048]{1,0:T(8,128)(2,1)S(1)}, bf16[384,2048]{1,0:T(8,128)(2,1)S(1)}, bf16[384,2048]{1,0:T(8,128)(2,1)S(1)}, f32[256,2048]{1,0:T(8,128)S(1)}) custom-call(bf16[384,2048]{1,0:T(8,128)(2,1)} %gl_h.1, bf16[384,2048]{1,0:T(8,128)(2,1)} %ul_h.1, bf16[384,2048]{1,0:T(8,128)(2,1)} %ge_h.1, bf16[384,2048]{1,0:T(8,128)(2,1)} %ue_h.1, ...), custom_call_target="tpu_custom_call" | custom-call | tf_op jit(solution)/shard_map/pallas_call | solution.py:681
  97.3 2.9 %shard_map.103 = (bf16[384,2048]{1,0:T(8,128)(2,1)}, bf16[384,2048]{1,0:T(8,128)(2,1)}, bf16[384,2048]{1,0:T(8,128)(2,1)}, f32[256,2048]{1,0:T(8,128)}) custom-call(bf16[384,2048]{1,0:T(8,128)(2,1)S(1)} %get-tuple-element.8.refs_0_, bf16[384,2048]{1,0:T(8,128)(2,1)S(1)} %get-tuple-element.9.refs_1_, bf16[384,2048]{1,0:T(8,128)(2,1)S(1)} %get-tuple-element.10.refs_2_, ...), custom_call_target="tpu_custom_call" | custom-call | tf_op jit(solution)/shard_map/pallas_call | solution.py:738

commit v4 on v3

--- a/solution.py
+++ b/solution.py
@@ -15,22 +15,22 @@
 LIMIT = 56 << 20
 CHUNKS = 2
 LEAD = 2
-AHEAD = (1, 3)
-SETTLE = (1, 1)
+AHEAD = (1, 1)
+SETTLE = (2, 0)
 START = (2, 1)
-LAG = (2, 5)
-USE_LAG = (5, 7)
-Y0 = 0
-Y1 = 1
-Y1H = 1
-F1 = (1, 0)
+LAG = (4, 4)
+USE_LAG = (7, 5)
+Y0 = 1
+Y1 = 2
+Y1H = 0
+F1 = (0, 0)
 RSFIRST = 1
-YI = 1
-HOLD = 1
+YI = -1
+HOLD = 0
 FP = (2, 2)
-FC = (2, 2)
-P1 = 5
-H0 = 7
+FC = (1, 1)
+P1 = 6
+H0 = 6
 TILE = 16
 
 

time: 100 us -> 99.6 us (level)
  no operation moved by 1% of the time
where the time goes in v4:
time: 99.6 us; the launch traced here: 99.4 us
  Pallas kernels  98.8 us (99%)
    pallas_call x1, Pallas kernels, per_device(): pl.pallas_call(functools.partial(kernel, n, n_tp, chunks, scale), out_sha...  95.9 us
    pallas_call x1, Pallas kernels, per_device(): pl.pallas_call(deliver, out_shape=tuple((jax.ShapeDtypeStruct(a.shape, a....  2.91 us

profile of v4, /device:TPU:0, one launch (start us, length us, event | category | flops | bytes accessed | tf_op | source)
XLA Modules:
  0.0 99.4 jit_solution(11203936177588977389)
XLA Ops:
  0.6 95.9 %shard_map.102 = (bf16[384,2048]{1,0:T(8,128)(2,1)S(1)}, bf16[384,2048]{1,0:T(8,128)(2,1)S(1)}, bf16[384,2048]{1,0:T(8,128)(2,1)S(1)}, f32[256,2048]{1,0:T(8,128)S(1)}) custom-call(bf16[384,2048]{1,0:T(8,128)(2,1)} %gl_h.1, bf16[384,2048]{1,0:T(8,128)(2,1)} %ul_h.1, bf16[384,2048]{1,0:T(8,128)(2,1)} %ge_h.1, bf16[384,2048]{1,0:T(8,128)(2,1)} %ue_h.1, ...), custom_call_target="tpu_custom_call" | custom-call | tf_op jit(solution)/shard_map/pallas_call | solution.py:681
  96.5 2.9 %shard_map.103 = (bf16[384,2048]{1,0:T(8,128)(2,1)}, bf16[384,2048]{1,0:T(8,128)(2,1)}, bf16[384,2048]{1,0:T(8,128)(2,1)}, f32[256,2048]{1,0:T(8,128)}) custom-call(bf16[384,2048]{1,0:T(8,128)(2,1)S(1)} %get-tuple-element.8.refs_0_, bf16[384,2048]{1,0:T(8,128)(2,1)S(1)} %get-tuple-element.9.refs_1_, bf16[384,2048]{1,0:T(8,128)(2,1)S(1)} %get-tuple-element.10.refs_2_, ...), custom_call_target="tpu_custom_call" | custom-call | tf_op jit(solution)/shard_map/pallas_call | solution.py:738

commit v5 on v4

--- a/solution.py
+++ b/solution.py
@@ -47,6 +47,8 @@
     third = max(rows * P1 // 256, 1) * 16
     head = max(rows * H0 // 256, 1) * 16
     tail = rows - head
+    cut = tail // 32 * 16
+    cuts = pl.ds(0, cut), pl.ds(cut, tail - cut)
     nz = n // 2
     hq = cols // 2
     width = hq // chunks
@@ -324,7 +326,8 @@
             device_id=target(ACROSS), device_id_type=MESH,
         )
 
-    first, second = halves = pl.ds(0, head), pl.ds(head, tail)
+    first, second = pl.ds(0, head), pl.ds(head, tail)
+    spans = first, pl.ds(head, cut), pl.ds(head + cut, tail - cut)
     mine, cross = pl.ds(0, tail), pl.ds(tail, tail)
     bulk = pl.ds(0, 2 * tail)
     rest = pl.ds(2 * tail, head)
@@ -340,15 +343,16 @@
     def z_arrived(way, c, to, stage):
         z_copy(way, c, to, stage, OTHER).wait_recv()
 
-    def yf_copy(c):
-        return pltpu.make_async_remote_copy(
-            src_ref=yfs.at[c], dst_ref=yfr.at[c], send_sem=yf_s.at[c], recv_sem=yf_r.at[c],
+    def yf_copy(c, part):
+        return pltpu.make_async_remote_copy(
+            src_ref=yfs.at[c, cuts[part], :], dst_ref=yfr.at[c, cuts[part], :],
+            send_sem=yf_s.at[part, c], recv_sem=yf_r.at[part, c],
             device_id=target(ACROSS), device_id_type=MESH,
         )
 
     def x_copy(c, stage):
         return pltpu.make_async_remote_copy(
-            src_ref=xs.at[c, halves[stage], :], dst_ref=xr.at[c, halves[stage], :],
+            src_ref=xs.at[c, spans[stage], :], dst_ref=xr.at[c, spans[stage], :],
             send_sem=x_s.at[stage, c], recv_sem=x_r.at[stage, c],
             device_id={"rep": other}, device_id_type=MESH,
         )
@@ -447,7 +451,8 @@
                 own[c, z, second, :] += before[mine, :].astype(F32)
 
         yfs[c] = opp[c, z].astype(BF16)
-        yf_copy(c).start()
+        for part in range(2):
+            yf_copy(c, part).start()
         y_copy(c, z).wait_recv()
         own[c, z, first, :] += yr[c, z].astype(F32)
         for way, there in sides:
@@ -461,16 +466,18 @@
         x_copy(c, 0).start()
 
     def finish_pair(c):
-        yf_copy(c).wait_recv()
-        own[c, z, second, :] += yfr[c].astype(F32)
-        xs[c, second, :] = own[c, z, second, :].astype(BF16)
-        x_copy(c, 1).start()
+        for part in range(2):
+            yf_copy(c, part).wait_recv()
+            span = spans[1 + part]
+            own[c, z, span, :] += yfr[c, cuts[part], :].astype(F32)
+            xs[c, span, :] = own[c, z, span, :].astype(BF16)
+            x_copy(c, 1 + part).start()
         lanes = pl.ds(pl.multiple_of(rep * hq + c * width, 128), width)
         gout[:, lanes] = gin[:, lanes] + own[c, z] * scale
 
     def finish_cross(c):
         lanes = pl.ds(pl.multiple_of(other * hq + c * width, 128), width)
-        for stage, span in ((0, first), (1, second)):
+        for stage, span in enumerate(spans):
             x_copy(c, stage).wait_recv()
             gout[span, lanes] = gin[span, lanes] + xr[c, span, :].astype(F32) * scale
 
@@ -640,9 +647,10 @@
     @pl.loop(0, chunks)
     def _(c):
         he_cross(c).wait_send()
-        yf_copy(c).wait_send()
-        x_copy(c, 0).wait_send()
-        x_copy(c, 1).wait_send()
+        for part in range(2):
+            yf_copy(c, part).wait_send()
+        for stage in range(3):
+            x_copy(c, stage).wait_send()
 
 
 def deliver(*refs):
@@ -724,10 +732,10 @@
                 dma((chunks, nz)),
                 dma((2, chunks, nz)),
                 dma((4, chunks, nz)),
-                dma((chunks,)),
-                dma((chunks,)),
                 dma((2, chunks)),
                 dma((2, chunks)),
+                dma((3, chunks)),
+                dma((3, chunks)),
                 dma((n_tp, n)),
                 dma((n_tp, n)),
             ],

time: 99.6 us -> 99.2 us (level)
  no operation moved by 1% of the time
where the time goes in v5:
time: 99.2 us; the launch traced here: 99 us
  Pallas kernels  98.4 us (99%)
    pallas_call x1, Pallas kernels, per_device(): pl.pallas_call(functools.partial(kernel, n, n_tp, chunks, scale), out_sha...  95.5 us
    pallas_call x1, Pallas kernels, per_device(): pl.pallas_call(deliver, out_shape=tuple((jax.ShapeDtypeStruct(a.shape, a....  2.91 us

profile of v5, /device:TPU:0, one launch (start us, length us, event | category | flops | bytes accessed | tf_op | source)
XLA Modules:
  0.0 99.0 jit_solution(18012484559154479570)
XLA Ops:
  0.6 95.5 %shard_map.102 = (bf16[384,2048]{1,0:T(8,128)(2,1)S(1)}, bf16[384,2048]{1,0:T(8,128)(2,1)S(1)}, bf16[384,2048]{1,0:T(8,128)(2,1)S(1)}, f32[256,2048]{1,0:T(8,128)S(1)}) custom-call(bf16[384,2048]{1,0:T(8,128)(2,1)} %gl_h.1, bf16[384,2048]{1,0:T(8,128)(2,1)} %ul_h.1, bf16[384,2048]{1,0:T(8,128)(2,1)} %ge_h.1, bf16[384,2048]{1,0:T(8,128)(2,1)} %ue_h.1, ...), custom_call_target="tpu_custom_call" | custom-call | tf_op jit(solution)/shard_map/pallas_call | solution.py:689
  96.1 2.9 %shard_map.103 = (bf16[384,2048]{1,0:T(8,128)(2,1)}, bf16[384,2048]{1,0:T(8,128)(2,1)}, bf16[384,2048]{1,0:T(8,128)(2,1)}, f32[256,2048]{1,0:T(8,128)}) custom-call(bf16[384,2048]{1,0:T(8,128)(2,1)S(1)} %get-tuple-element.8.refs_0_, bf16[384,2048]{1,0:T(8,128)(2,1)S(1)} %get-tuple-element.9.refs_1_, bf16[384,2048]{1,0:T(8,128)(2,1)S(1)} %get-tuple-element.10.refs_2_, ...), custom_call_target="tpu_custom_call" | custom-call | tf_op jit(solution)/shard_map/pallas_call | solution.py:746
